TPU v7x, 512 devices: a whole 4x4x16 slice. The times are simulated.
512 devices in a mesh: tp: 512 (over z, y, x, core).
Axes of the slice: x: 4, y: 4, z: 16, core: 2. Of those that a mesh axis runs over, the one named last changes fastest.
Arguments:
- tokens: bfloat16 [4096, 256], P('tp'), may hold values from -20 to 20, as said below
- positions: int32 [256], replicated, may hold values from 1 to 3072, 262144 in all
- norm_gain: float32 [4096], replicated, may hold values from 0.1 to 1.9
- w_query: bfloat16 [1024, 4096], P('tp'), may hold values from -0.09375 to 0.09375
- w_key: bfloat16 [1024, 4096], P('tp'), may hold values from -0.09375 to 0.09375
- w_value: bfloat16 [2048, 4096], P('tp'), may hold values from -0.09375 to 0.09375
- w_outgate: bfloat16 [2048, 4096], P('tp'), may hold values from -0.09375 to 0.09375
- w_input: bfloat16 [4, 4096], replicated, may hold values from -0.09375 to 0.09375
- w_forget: bfloat16 [4, 4096], replicated, may hold values from -0.09375 to 0.09375
- bias_input: float32 [4], replicated, may hold values from -3 to 3
- bias_forget: float32 [4], replicated, may hold values from -1 to 4
- w_read: bfloat16 [4096, 2048], P('tp'), may hold values from -0.125 to 0.125
- cells: float32 [2048, 256, 256], P('tp'), may hold values from -4 to 4
- norms: float32 [1024, 256], replicated, may hold values from 0 to 0.5
- maxima: float32 [4, 256], replicated, may hold values from -1 to 1
Outputs:
- mixed_rows: bfloat16 [4096, 256], P('tp')
- new_cells: float32 [2048, 256, 256], P('tp')
- new_norms: float32 [1024, 256], replicated
- new_maxima: float32 [4, 256], replicated
Inputs may be any that keep to these rules, and one draw needn't show every extreme that they name: `tokens`: feature rows have their own scales, spread over a factor of ten.
All inputs are finite; a program needn't handle non-finite values.
Results may differ from a plain program's by a relative error of at most 0.0062.
The roundings to bfloat16 on the way count: a program that leaves them out, or rounds other values in their place, can miss the bound.
Values may be sent and summed in bfloat16 or wider, within the bound.
A program may use at most 64 MiB of HBM per device.

v0:
```python
import functools

import jax
import jax.numpy as jnp
from jax import lax
from jax.sharding import Mesh
from jax.sharding import PartitionSpec as P

DQK = 256
MOST_LEN = 3072
TP = ("tp_0", "tp_1", "tp_2", "tp_3")


EPS = 1e-06


def one_axis_at_a_time(shard, axes):
    return functools.reduce(lax.psum, axes, shard)


def joined_along(parts, dim):
    parts = jnp.moveaxis(parts, 0, dim)
    shape = parts.shape
    return parts.reshape(*shape[:dim], shape[dim] * shape[dim + 1], *shape[dim + 2 :])


def stacked_from(shard, axes, order):
    parts = shard
    for k in order:
        parts = lax.all_gather(parts, axes[k])
    done = order[::-1]
    back = [done.index(k) for k in range(len(axes))]
    parts = parts.transpose(*back, *range(len(axes), parts.ndim))
    return parts.reshape(-1, *shard.shape)


def whole_of(shard, axes, order, dim):
    return joined_along(stacked_from(shard, axes, order), dim)


def in_one_piece(arrays, axis, dim, along):
    both = jnp.concatenate(arrays, axis=along)
    whole, at, gathered = (lax.all_gather(both, axis, axis=dim, tiled=True), 0, [])
    for a in arrays:
        gathered.append(lax.slice_in_dim(whole, at, at + a.shape[along], axis=along))
        at += a.shape[along]
    return tuple(gathered)


def mix_block(
    rows,
    where,
    gain,
    w_query,
    w_key,
    w_value,
    w_outgate,
    w_input,
    w_forget,
    bias_input,
    bias_forget,
    w_read,
    cells,
    norms,
    maxima,
):
    count = lax.axis_size(TP)
    index = lax.axis_index(TP)
    seqs = rows.shape[1]
    width_loc = rows.shape[0]
    model_width = gain.shape[0]
    heads = w_input.shape[0]
    head = index * heads // count
    own_gain = lax.dynamic_slice_in_dim(gain, index * width_loc, width_loc)
    local_rows = rows.astype(jnp.float32)
    total = one_axis_at_a_time(jnp.sum(local_rows * local_rows, axis=0), TP)
    normed = whole_of(
        (local_rows * own_gain[:, None]).astype(jnp.bfloat16),
        (("tp_0", "tp_1", "tp_2"), "tp_3"),
        (0, 1),
        0,
    )
    scale = lax.rsqrt(total / model_width + EPS)[None, :]
    query_loc = (jnp.dot(w_query, normed, preferred_element_type=jnp.float32) * scale).astype(
        jnp.bfloat16
    )
    key_loc = (
        jnp.dot(w_key, normed, preferred_element_type=jnp.float32) * scale * DQK ** (-0.5)
    ).astype(jnp.bfloat16)
    query_all, key_all = in_one_piece((query_loc, key_loc), TP, 0, 1)
    value = jnp.dot(w_value, normed, preferred_element_type=jnp.float32) * scale
    outgate = jnp.dot(w_outgate, normed, preferred_element_type=jnp.float32) * scale
    gate_in = (
        jnp.dot(w_input, normed, preferred_element_type=jnp.float32) * scale + bias_input[:, None]
    )
    gate_forget = (
        jnp.dot(w_forget, normed, preferred_element_type=jnp.float32) * scale + bias_forget[:, None]
    )
    logf = jax.nn.log_sigmoid(gate_forget) * (1.0 + where / MOST_LEN)
    new_max = jnp.maximum(logf + maxima, gate_in)
    decay = jnp.exp(logf + maxima - new_max)
    fresh = jnp.exp(gate_in - new_max)
    queries = query_all.astype(jnp.float32).reshape(heads, DQK, seqs)
    keys = key_all.astype(jnp.float32).reshape(heads, DQK, seqs)
    norms_new = decay[:, None, :] * norms.reshape(heads, DQK, seqs) + fresh[:, None, :] * keys
    denom = jnp.sum(queries * norms_new, axis=1)
    decay_own = lax.dynamic_index_in_dim(decay, head, 0)
    fresh_own = lax.dynamic_index_in_dim(fresh, head, 0)
    den_own = lax.dynamic_index_in_dim(denom, head, 0)
    q_head = lax.dynamic_slice_in_dim(query_all, head * DQK, DQK, 0).astype(jnp.float32)
    k_head = lax.dynamic_slice_in_dim(key_all, head * DQK, DQK, 0).astype(jnp.float32)
    new_cells = decay_own[None] * cells + fresh_own[None] * value[:, None, :] * k_head[None, :, :]
    numer = jnp.sum(q_head[None, :, :] * new_cells, axis=1)
    hidden = numer / jnp.maximum(jnp.abs(den_own), 1.0)
    gated = (hidden * jax.nn.sigmoid(outgate)).astype(jnp.bfloat16)
    mixed = jnp.dot(
        w_read, whole_of(gated, TP, (0, 1, 2, 3), 0), preferred_element_type=jnp.float32
    )
    new_rows = (rows.astype(jnp.float32) + mixed).astype(jnp.bfloat16)
    return (new_rows, new_cells, norms_new.reshape(heads * DQK, seqs), new_max)


def shards(
    tokens,
    positions,
    norm_gain,
    w_query,
    w_key,
    w_value,
    w_outgate,
    w_input,
    w_forget,
    bias_input,
    bias_forget,
    w_read,
    cells,
    norms,
    maxima,
):
    row_parts, cell_parts, norm_parts, max_parts = ([], [], [], [])
    where = positions.astype(jnp.float32)[None, :]
    rows, cell_new, norm_new, max_new = mix_block(
        tokens,
        where,
        norm_gain,
        w_query,
        w_key,
        w_value,
        w_outgate,
        w_input,
        w_forget,
        bias_input,
        bias_forget,
        w_read,
        cells,
        norms,
        maxima,
    )
    row_parts.append(rows)
    cell_parts.append(cell_new)
    norm_parts.append(norm_new)
    max_parts.append(max_new)
    return (row_parts[0], cell_parts[0], norm_parts[0], max_parts[0])


def solution(mesh):
    finer = Mesh(mesh.devices.reshape(16, 4, 4, 2), ("tp_0", "tp_1", "tp_2", "tp_3"))
    return jax.shard_map(
        shards,
        mesh=finer,
        in_specs=(
            P(TP, None),
            P(),
            P(),
            P(TP, None),
            P(TP, None),
            P(TP, None),
            P(TP, None),
            P(),
            P(),
            P(),
            P(),
            P(TP, None),
            P(TP, None, None),
            P(),
            P(),
        ),
        out_specs=(P(TP, None), P(TP, None, None), P(), P()),
        check_vma=False,
    )
```

profile of v0, /device:TPU:1, one launch (start us, length us, event | category | flops | bytes accessed | tf_op | source)
XLA Modules:
  0.0 513.4 jit_solution(18150187819339620999)
XLA Ops:
  7.2 0.8 dynamic_slice.19
  8.0 1.4 fusion.25
  9.4 191.6 %all-gather.13.cloned.1.call-done = bf16[2048,256]{1,0:T(8,128)(2,1)} async-done(((bf16[8,256]{1,0:T(8,128)(2,1)}), bf16[2048,256]{1,0:T(8,128)(2,1)}) %all-gather.13.cloned.1.call-update) | async-done | bytes 1048592 | tf_op jit(solution)/shard_map/all_gather | solution.py:30
  201.1 21.8 %psum.28 = f32[256]{0:T(256)S(1)} all-reduce(f32[256]{0:T(256)S(1)} %get-tuple-element.10), channel_id=1, replica_groups=mesh['tp_0'=16,'tp_1'=4,'tp_2'=4,'tp_3'=2] {'tp_0'}, use_global_device_ids=true, to_apply=%region_1.2 | all-reduce | flops 256 | bytes 2048 | tf_op jit(solution)/shard_map/psum | solution.py:18
  222.9 8.8 %psum.29 = f32[256]{0:T(256)S(1)} all-reduce(f32[256]{0:T(256)S(1)} %psum.28), channel_id=1, replica_groups=mesh['tp_0'=16,'tp_1'=4,'tp_2'=4,'tp_3'=2] {'tp_1'}, use_global_device_ids=true, to_apply=%region_2.3 | all-reduce | flops 256 | bytes 2048 | tf_op jit(solution)/shard_map/psum | solution.py:18
  231.7 9.6 %psum.30 = f32[256]{0:T(256)S(1)} all-reduce(f32[256]{0:T(256)S(1)} %psum.29), channel_id=1, replica_groups=mesh['tp_0'=16,'tp_1'=4,'tp_2'=4,'tp_3'=2] {'tp_2'}, use_global_device_ids=true, to_apply=%region_3.4 | all-reduce | flops 256 | bytes 2048 | tf_op jit(solution)/shard_map/psum | solution.py:18
  241.3 23.9 %psum.31 = f32[256]{0:T(256)S(1)} all-reduce(f32[256]{0:T(256)S(1)} %psum.30), channel_id=1, replica_groups=mesh['tp_0'=16,'tp_1'=4,'tp_2'=4,'tp_3'=2] {'tp_3'}, use_global_device_ids=true, to_apply=%region_4.5 | all-reduce | flops 256 | bytes 2048 | tf_op jit(solution)/shard_map/psum | solution.py:18
  265.2 1.8 copy.22
  268.1 0.6 maximum_bitcast_fusion
  269.2 0.4 subtract_exponential_fusion.1
  269.7 158.9 %all-gather.19.cloned.1.call-done = bf16[512,2,512]{2,1,0:T(2,128)(2,1)} async-done(((bf16[1,2,512]{2,1,0:T(2,128)(2,1)}), bf16[512,2,512]{2,1,0:T(2,128)(2,1)}) %all-gather.19.cloned.1.call-update) | async-done | bytes 1048592 | tf_op jit(solution)/shard_map/all_gather | solution.py:43
  428.6 1.5 reshape.53
  430.1 1.5 fusion.22
  431.7 0.4 fusion.9
  432.1 0.8 copy-done.1
  432.9 1.1 multiply_reduce_fusion
  434.0 0.4 fusion.16
  434.4 20.9 %all-gather.7 = bf16[16,4,256]{2,1,0:T(4,128)(2,1)S(1)} all-gather(bf16[1,4,256]{2,1,0:T(4,128)(2,1)S(1)} %fusion.16), channel_id=4, replica_groups=mesh['tp_0'=16,'tp_1'=4,'tp_2'=4,'tp_3'=2] {'tp_0'}, dimensions={0}, use_global_device_ids=true | all-gather | bytes 34816 | tf_op jit(solution)/shard_map/all_gather | solution.py:30
  455.3 9.4 %all-gather.3 = bf16[64,4,256]{2,1,0:T(4,128)(2,1)S(1)} all-gather(bf16[16,4,256]{2,1,0:T(4,128)(2,1)S(1)} %all-gather.7), channel_id=5, replica_groups=mesh['tp_0'=16,'tp_1'=4,'tp_2'=4,'tp_3'=2] {'tp_1'}, dimensions={0}, use_global_device_ids=true | all-gather | bytes 163840 | tf_op jit(solution)/shard_map/all_gather | solution.py:30
  464.8 11.1 %all-gather.4 = bf16[16,16,4,256]{3,1,2,0:T(8,128)(2,1)} all-gather(bf16[4,16,4,256]{3,1,2,0:T(8,128)(2,1)S(1)} %copy.23), channel_id=6, replica_groups=mesh['tp_0'=16,'tp_1'=4,'tp_2'=4,'tp_3'=2] {'tp_2'}, dimensions={0}, use_global_device_ids=true | all-gather | bytes 655360 | tf_op jit(solution)/shard_map/all_gather | solution.py:30
  476.0 2.3 fusion.23
  478.3 25.6 %all-gather.17.cloned.1.call-done = bf16[8,4,16,4,256]{4,2,3,1,0:T(8,128)(2,1)} async-done(((bf16[4,4,16,4,256]{4,2,3,1,0:T(8,128)(2,1)}), bf16[8,4,16,4,256]{4,2,3,1,0:T(8,128)(2,1)}) %all-gather.17.cloned.1.call-update) | async-done | bytes 1048592 | tf_op jit(solution)/shard_map/all_gather | solution.py:30
  503.9 1.8 copy.24
  506.0 0.8 fusion.1
  (48 shorter events, 2.2 us)
Async XLA Ops:
  7.2 262.0 %copy-start = (bf16[4,4096]{1,0:T(4,128)(2,1)S(1)}, bf16[4,4096]{1,0:T(4,128)(2,1)}, u32[]{:S(2)}) copy-start(bf16[4,4096]{1,0:T(4,128)(2,1)} %param.23) | copy-start | bytes 98308
  7.2 193.9 %all-gather.13.cloned.1.call-start = ((), (), s32[]{:S(2)}) async-start(), calls=%async_computation | async-start | bytes 1052672 | tf_op jit(solution)/shard_map/all_gather | solution.py:30
  9.4 255.8 %all-gather.15.cloned.1.call-start = ((), (), s32[]{:S(2)}) async-start(), calls=%async_computation.1 | async-start | bytes 3145728 | tf_op jit(solution)/shard_map/all_gather | solution.py:30
  201.1 227.5 %all-gather.19.cloned.1.call-start = ((), (), s32[]{:S(2)}) async-start(), calls=%async_computation.3 | async-start | bytes 1050624 | tf_op jit(solution)/shard_map/all_gather | solution.py:43
  265.2 1.8 copy-start.6
  267.0 0.7 copy-start.7
  267.0 1.8 copy-start.13
  267.0 1.8 copy-start.2
  267.0 1.8 copy-start.11
  267.7 1.5 copy-start.10
  267.7 1.5 copy-start.12
  268.7 235.2 %all-gather.17.cloned.1.call-start = ((), (), s32[]{:S(2)}) async-start(), calls=%async_computation.2 | async-start | bytes 1572864 | tf_op jit(solution)/shard_map/all_gather | solution.py:30
  269.6 162.0 %copy-start.8 = (f32[4,256]{1,0:T(4,128)}, f32[4,256]{1,0:T(4,128)S(1)}, u32[]{:S(2)}) copy-start(f32[4,256]{1,0:T(4,128)S(1)} %get-tuple-element.9) | copy-start | bytes 12292
  430.1 1.6 copy-start.3
  431.7 1.2 copy-start.1
  432.1 1.9 copy-start.4
  503.9 2.1 copy-start.5
  503.9 2.1 copy-start.9
Sparse Core Ops, SparseCore 0:
  12.8 188.1 all-gather.12
  203.1 29.5 all-gather.14
  268.8 159.7 all-gather.18
  476.1 27.7 all-gather.16
where the time goes:
time: 514 us; the launch traced here: 513 us
  waiting for transfers between devices  376 us (73%)
  blocking collectives  106 us (21%)
  between operations  14 us (3%)
  local copies, waits for them, and re-layouts  7.26 us (1%)
  other arithmetic  7 us (1%)
    all_gather x3, waiting for transfers between devices, stacked_from(): parts = lax.all_gather(parts, axes[k])  217 us
    all_gather x1, waiting for transfers between devices, in_one_piece(): lax.all_gather(both, axis, axis=dim, tiled=True)  159 us
    psum x4, blocking collectives, one_axis_at_a_time(): return functools.reduce(lax.psum, axes, shard)  64 us
    all_gather x3, blocking collectives, stacked_from(): parts = lax.all_gather(parts, axes[k])  41.5 us
  transfers between devices with their start and end apart: 4, of which 3 were waited for; matrix products, arithmetic and copies ran while one was open for 1% of the time, Pallas kernels for 0%

commit v1 on v0

v1 whole, which is shorter than its diff:
```python
import functools

import jax
import jax.numpy as jnp
from jax import lax
from jax.experimental import pallas as pl
from jax.experimental.pallas import tpu as pltpu
from jax.sharding import PartitionSpec as P

DQK = 256
MOST_LEN = 3072
EPS = 1e-06
NZ, NY, NX, NC = 16, 4, 4, 2
CUBE = 4
F32 = jnp.float32
BF16 = jnp.bfloat16
MESH = pl.DeviceIdType.MESH


def kernel(
    tokens,
    *refs,
):
    sources, (rows_out, cells_v, norms_v, max_out), rest = refs[:14], refs[14:18], refs[18:]
    held, rest = rest[:12], rest[12:]
    body(tokens, sources, held, rows_out, cells_v, norms_v, max_out, *rest)


def body(
    tokens,
    sources,
    held,
    rows_out,
    cells_v,
    norms_v,
    max_out,
    tok,
    gbuf,
    kq,
    weights,
    gain_b,
    qf,
    kf,
    dec,
    fre,
    local_sem,
    z_s,
    z_r,
    p1_s,
    p1_r,
    p2_s,
    p2_r,
    d_s,
    d_r,
    qz_s,
    qz_r,
    qy_s,
    qy_r,
    qx_s,
    qx_r,
    qd_s,
    qd_r,
):
    me = lax.axis_index("tp")
    core = me % NC
    x = (me // NC) % NX
    y = (me // (NC * NX)) % NY
    z = me // (NC * NX * NY)
    head = z // CUBE
    zlo = z % CUBE

    def device(zz, yy, xx, cc):
        return (((zz * NY + yy) * NX + xx) * NC + cc,)

    def send(ref, dst, ss, rs, to):
        return pltpu.make_async_remote_copy(
            src_ref=ref, dst_ref=dst, send_sem=ss, recv_sem=rs, device_id=to, device_id_type=MESH
        )

    loads = [
        pltpu.make_async_copy(
            tokens.at[:, pl.ds(128 * half, 128)], tok.at[half, z, y, x, core], local_sem.at[half]
        )
        for half in range(2)
    ]
    (where_ref, gain_ref, wq_ref, wk_ref, wv_ref, wo_ref, wi_ref, wf_ref) = held[:8]
    (bi_ref, bf_ref, wr_ref, maxima_ref) = held[8:]
    targets = held[:11] + (cells_v, norms_v, maxima_ref)
    for i, (source, target) in enumerate(zip(sources, targets)):
        loads.append(pltpu.make_async_copy(source, target, local_sem.at[2 + i]))
    for copy in loads:
        copy.start()

    barrier = pltpu.get_barrier_semaphore()

    def greet(to):
        pl.semaphore_signal(barrier, inc=1, device_id=to, device_id_type=MESH)

    @pl.loop(1, NZ)
    def _(dz):
        greet(device((z + dz) % NZ, y, x, core))

    @pl.loop(1, NY)
    def _(dy):
        greet(device(z, (y + dy) % NY, x, core))

    @pl.loop(1, NX)
    def _(dx):
        greet(device(z, y, (x + dx) % NX, core))

    greet(device(z, y, x, 1 - core))

    for i in (1, 2, 3, 4, 5, 6, 7):
        loads[2 + i].wait()

    weights[...] = jnp.zeros_like(weights)
    weights[0:2, :] = wq_ref[...]
    weights[2:4, :] = wk_ref[...]
    weights[4:8, :] = wv_ref[...]
    weights[8:12, :] = wo_ref[...]
    weights[12:16, :] = wi_ref[...]
    weights[16:20, :] = wf_ref[...]
    gain_t = gain_ref[...].T
    for r in range(2 * NZ):
        gain_b[r // 2, 128 * (r % 2) : 128 * (r % 2 + 1)] = jnp.broadcast_to(
            gain_t[:, r : r + 1], (128, 128)
        )

    pl.semaphore_wait(barrier, NZ - 1 + NY - 1 + NX - 1 + 1)
    for i in (0, 1, 2, 10, 11, 12, 15):
        loads[i].wait()

    def z_copy(buf, n, dz):
        mine = buf.at[:, z, y, x, core]
        return send(mine, mine, z_s.at[n, dz], z_r.at[n, dz], device((z + dz) % NZ, y, x, core))

    def first_copy(buf, n, half, d):
        mine = buf.at[half, :, y, x, core]
        to = device(z, (y + d) % NY, x, core) if half == 0 else device(z, y, (x + d) % NX, core)
        return send(mine, mine, p1_s.at[n, half, d], p1_r.at[n, half, d], to)

    def second_copy(buf, n, half, d):
        if half == 0:
            mine = buf.at[half, :, :, x, core]
            to = device(z, y, (x + d) % NX, core)
        else:
            mine = buf.at[half, :, y, :, core]
            to = device(z, (y + d) % NY, x, core)
        return send(mine, mine, p2_s.at[n, half, d], p2_r.at[n, half, d], to)

    def core_copy(buf, n, half, d):
        if half == 0:
            part = buf.at[half, :, :, (x + NX - d) % NX, core]
        else:
            part = buf.at[half, :, (y + NY - d) % NY, :, core]
        return send(part, part, d_s.at[n, half, d], d_r.at[n, half, d], device(z, y, x, 1 - core))

    def start_z(buf, n):
        @pl.loop(0, NZ - 1)
        def _(i):
            dz = 8 + ((i + 1) // 2) * (2 * (i % 2) - 1)
            z_copy(buf, n, dz).start()

    def finish_z(buf, n):
        @pl.loop(1, NZ)
        def _(dz):
            z_copy(buf, n, dz).wait_recv()

    def start_first(buf, n):
        for d in (2, 1, 3):
            for half in range(2):
                first_copy(buf, n, half, d).start()

    def second(buf, n):
        for half in range(2):
            for d in (1, 3, 2):
                first_copy(buf, n, half, d).wait_recv()
            for d in (2, 1, 3):
                second_copy(buf, n, half, d).start()
        for half in range(2):
            core_copy(buf, n, half, 0).start()
        for d in (1, 3, 2):
            for half in range(2):
                second_copy(buf, n, half, d).wait_recv()
                core_copy(buf, n, half, d).start()

    def finish_core(buf, n):
        for half in range(2):
            for d in range(4):
                core_copy(buf, n, half, d).wait_recv()

    def drain(buf, n):
        @pl.loop(1, NZ)
        def _(dz):
            z_copy(buf, n, dz).wait_send()

        for half in range(2):
            for d in range(1, 4):
                first_copy(buf, n, half, d).wait_send()
                second_copy(buf, n, half, d).wait_send()
            for d in range(4):
                core_copy(buf, n, half, d).wait_send()

    start_z(tok, 0)
    finish_z(tok, 0)
    start_first(tok, 0)
    second(tok, 0)
    finish_core(tok, 0)

    def project(i, carry):
        acc, squares = carry
        halves = []
        sums = []
        for half in range(2):
            t = tok[half, i].astype(F32).reshape(256, 128)
            sums.append(jnp.sum((t * t).reshape(32, 8, 128), axis=0))
            halves.append((t * gain_b[i]).astype(BF16))
        normed = jnp.concatenate(halves, axis=1)
        w = weights[:, pl.ds(pl.multiple_of(i * 256, 256), 256)]
        acc = acc + jnp.dot(w, normed, preferred_element_type=F32)
        return acc, squares + jnp.concatenate(sums, axis=1)

    acc, squares = lax.fori_loop(
        0, NZ, project, (jnp.zeros((32, 256), F32), jnp.zeros((8, 256), F32))
    )
    total = jnp.sum(squares, axis=0, keepdims=True)
    scale = lax.rsqrt(total / (NZ * NY * NX * NC * 8) + EPS)
    proj = acc * scale
    query = proj[0:2].astype(BF16)
    key = (proj[2:4] * DQK ** (-0.5)).astype(BF16)
    for half in range(2):
        kq[z, y, x, core, half] = key[:, 128 * half : 128 * (half + 1)]
        kq[z, y, x, core, 2 + half] = query[:, 128 * half : 128 * (half + 1)]

    def qz_copy(dz):
        mine = kq.at[z, y, x, core]
        to = device(head * CUBE + (zlo + dz) % CUBE, y, x, core)
        return send(mine, mine, qz_s.at[0, dz], qz_r.at[0, dz], to)

    def kz_copy(dh, j):
        mine = kq.at[z, y, x, core, pl.ds(0, 2)]
        to = device(((head + dh) % 4) * CUBE + (zlo + j) % CUBE, y, x, core)
        return send(mine, mine, qz_s.at[dh, j], qz_r.at[dh, j], to)

    def zs_of(dh):
        return pl.ds(((head + 4 - dh) % 4) * CUBE, CUBE)

    def parts(dh):
        return pl.ds(0, 4 if dh == 0 else 2)

    def qy_copy(dh, d):
        mine = kq.at[zs_of(dh), y, x, core, parts(dh)]
        to = device(z, (y + d) % NY, x, core)
        return send(mine, mine, qy_s.at[dh, d], qy_r.at[dh, d], to)

    def qx_copy(dh, d):
        mine = kq.at[zs_of(dh), :, x, core, parts(dh)]
        to = device(z, y, (x + d) % NX, core)
        return send(mine, mine, qx_s.at[dh, d], qx_r.at[dh, d], to)

    def qd_copy(dh, d):
        part = kq.at[zs_of(dh), :, (x + NX - d) % NX, core, parts(dh)]
        to = device(z, y, x, 1 - core)
        return send(part, part, qd_s.at[dh, d], qd_r.at[dh, d], to)

    for dz in (2, 1, 3):
        qz_copy(dz).start()
    for dh in (2, 1, 3):
        for j in range(CUBE):
            kz_copy(dh, j).start()

    value = proj[4:8]
    outgate = jax.nn.sigmoid(proj[8:12])
    length = 1.0 + where_ref[...].astype(F32) / MOST_LEN
    for h in range(4):
        gate_in = proj[12 + h : 13 + h] + bi_ref[h]
        forget = proj[16 + h : 17 + h] + bf_ref[h]
        logf = (jnp.minimum(forget, 0.0) - jnp.log1p(jnp.exp(-jnp.abs(forget)))) * length
        held = logf + maxima_ref[h : h + 1]
        new_max = jnp.maximum(held, gate_in)
        max_out[h : h + 1] = new_max
        dec[h] = jnp.exp(held - new_max)
        fre[h] = jnp.exp(gate_in - new_max)

    for dz in (1, 3, 2):
        qz_copy(dz).wait_recv()
    for d in (2, 1, 3):
        qy_copy(0, d).start()
    for d in (1, 3, 2):
        qy_copy(0, d).wait_recv()
    for d in (2, 1, 3):
        qx_copy(0, d).start()
    qd_copy(0, 0).start()
    for d in (1, 3, 2):
        qx_copy(0, d).wait_recv()
        qd_copy(0, d).start()
    for dh in range(1, 4):
        for j in range(CUBE):
            kz_copy(dh, j).wait_recv()
        for d in (2, 1, 3):
            qy_copy(dh, d).start()
    for d in range(4):
        qd_copy(0, d).wait_recv()

    for half in range(2):
        lanes = slice(128 * half, 128 * (half + 1))
        kf[:, lanes] = kq[zs_of(0), :, :, :, half].astype(F32).reshape(DQK, 128)
        qf[:, lanes] = kq[zs_of(0), :, :, :, 2 + half].astype(F32).reshape(DQK, 128)
    loads[13].wait()
    loads[14].wait()
    decay = dec[head]
    fresh = fre[head]
    fv = fresh * value

    def memory(i, carry):
        at = pl.ds(pl.multiple_of(i * 16, 16), 16)
        q, k = qf[at], kf[at]
        own = norms_v[pl.ds(pl.multiple_of(head * DQK + i * 16, 16), 16)]
        out = []
        for v in range(4):
            new = decay * cells_v[v, at] + fv[v : v + 1] * k
            cells_v[v, at] = new
            prod = q * new
            out.append(carry[v] + prod[0:8] + prod[8:16])
        prod = q * (decay * own + fresh * k)
        out.append(carry[4] + prod[0:8] + prod[8:16])
        return tuple(out)

    sums = lax.fori_loop(0, DQK // 16, memory, (jnp.zeros((8, 256), F32),) * 5)
    denom = jnp.sum(sums[4], axis=0, keepdims=True)
    numer = jnp.concatenate([jnp.sum(sums[v], axis=0, keepdims=True) for v in range(4)], axis=0)
    hidden = numer / jnp.maximum(jnp.abs(denom), 1.0)
    gated = (hidden * outgate).astype(BF16)
    for half in range(2):
        gbuf[half, z, y, x, core] = gated[:, 128 * half : 128 * (half + 1)]

    start_z(gbuf, 1)
    for dh in range(1, 4):
        for d in (1, 3, 2):
            qy_copy(dh, d).wait_recv()
        for d in (2, 1, 3):
            qx_copy(dh, d).start()
        qd_copy(dh, 0).start()
    finish_z(gbuf, 1)
    start_first(gbuf, 1)
    for dh in range(1, 4):
        for d in (1, 3, 2):
            qx_copy(dh, d).wait_recv()
            qd_copy(dh, d).start()
    second(gbuf, 1)

    for dh in range(1, 4):
        for d in range(4):
            qd_copy(dh, d).wait_recv()

    @pl.loop(0, 4)
    def _(h):
        rows = pl.ds(pl.multiple_of(h * DQK, DQK), DQK)
        for half in range(2):
            lanes = slice(128 * half, 128 * (half + 1))
            k = kq[pl.ds(h * CUBE, CUBE), :, :, :, half].astype(F32).reshape(DQK, 128)
            norms_v[rows, lanes] = dec[h][:, lanes] * norms_v[rows, lanes] + fre[h][:, lanes] * k

    finish_core(gbuf, 1)
    total_rows = NZ * NY * NX * NC * 4
    for half in range(2):
        g = gbuf[half].reshape(total_rows, 128)
        mixed = jnp.dot(wr_ref[...], g, preferred_element_type=F32)
        lanes = slice(128 * half, 128 * (half + 1))
        rows_out[:, lanes] = (tok[half, z, y, x, core].astype(F32) + mixed).astype(BF16)

    drain(tok, 0)
    drain(gbuf, 1)
    for dz in range(1, 4):
        qz_copy(dz).wait_send()
    for dh in range(1, 4):
        for j in range(CUBE):
            kz_copy(dh, j).wait_send()
    for dh in range(4):
        for d in range(1, 4):
            qy_copy(dh, d).wait_send()
            qx_copy(dh, d).wait_send()
        for d in range(4):
            qd_copy(dh, d).wait_send()


def step(
    tokens,
    positions,
    norm_gain,
    w_query,
    w_key,
    w_value,
    w_outgate,
    w_input,
    w_forget,
    bias_input,
    bias_forget,
    w_read,
    cells,
    norms,
    maxima,
):
    vmem = pl.BlockSpec(memory_space=pltpu.VMEM)
    dma = pltpu.SemaphoreType.DMA
    return pl.pallas_call(
        kernel,
        out_shape=(
            jax.ShapeDtypeStruct((8, 256), BF16),
            jax.ShapeDtypeStruct((4, 256, 256), F32),
            jax.ShapeDtypeStruct((1024, 256), F32),
            jax.ShapeDtypeStruct((4, 256), F32),
        ),
        in_specs=[pl.BlockSpec(memory_space=pltpu.HBM)] * 15,
        out_specs=(vmem,) * 4,
        scratch_shapes=[
            pltpu.VMEM((1, 256), jnp.int32),
            pltpu.VMEM((32, 128), F32),
            pltpu.VMEM((2, 4096), BF16),
            pltpu.VMEM((2, 4096), BF16),
            pltpu.VMEM((4, 4096), BF16),
            pltpu.VMEM((4, 4096), BF16),
            pltpu.VMEM((4, 4096), BF16),
            pltpu.VMEM((4, 4096), BF16),
            pltpu.SMEM((4,), F32),
            pltpu.SMEM((4,), F32),
            pltpu.VMEM((8, 2048), BF16),
            pltpu.VMEM((4, 256), F32),
            pltpu.VMEM((2, NZ, NY, NX, NC, 8, 128), BF16),
            pltpu.VMEM((2, NZ, NY, NX, NC, 4, 128), BF16),
            pltpu.VMEM((NZ, NY, NX, NC, 4, 2, 128), BF16),
            pltpu.VMEM((32, 4096), BF16),
            pltpu.VMEM((NZ, 256, 128), F32),
            pltpu.VMEM((256, 256), F32),
            pltpu.VMEM((256, 256), F32),
            pltpu.VMEM((4, 1, 256), F32),
            pltpu.VMEM((4, 1, 256), F32),
            dma((16,)),
            dma((2, 16)),
            dma((2, 16)),
            dma((2, 2, 4)),
            dma((2, 2, 4)),
            dma((2, 2, 4)),
            dma((2, 2, 4)),
            dma((2, 2, 4)),
            dma((2, 2, 4)),
            dma((4, 4)),
            dma((4, 4)),
            dma((4, 4)),
            dma((4, 4)),
            dma((4, 4)),
            dma((4, 4)),
            dma((4, 4)),
            dma((4, 4)),
        ],
        compiler_params=pltpu.CompilerParams(
            collective_id=0, has_side_effects=True, vmem_limit_bytes=64700000
        ),
    )(
        tokens,
        positions.reshape(1, 256),
        norm_gain.reshape(32, 128),
        w_query,
        w_key,
        w_value,
        w_outgate,
        w_input,
        w_forget,
        bias_input,
        bias_forget,
        w_read,
        cells,
        norms,
        maxima,
    )


def solution(mesh):
    return jax.shard_map(
        step,
        mesh=mesh,
        in_specs=(
            P("tp", None),
            P(),
            P(),
            P("tp", None),
            P("tp", None),
            P("tp", None),
            P("tp", None),
            P(),
            P(),
            P(),
            P(),
            P("tp", None),
            P("tp", None, None),
            P(),
            P(),
        ),
        out_specs=(P("tp", None), P("tp", None, None), P(), P()),
        check_vma=False,
    )
```

time: 514 us -> 77.8 us (0.15)
  waiting for transfers between devices: 376 us -> 0 us
  blocking collectives: 106 us -> 0 us
  Pallas kernels: 0 us -> 71.8 us
  between operations: 14 us -> 0.66 us
  other arithmetic: 7 us -> 0 us
    all_gather x4 -> x0, waiting for transfers between devices: 376 us -> none  [the longest x3 217 us: stacked_from(): parts = lax.all_gather(parts, axes[k])]
    pallas_call x0 -> x1, Pallas kernels: none -> 71.8 us  [step(): pl.pallas_call(kernel, out_shape=(jax.ShapeDtypeStruct((8, 256), BF16), j...]
    psum x4 -> x0, blocking collectives: 64 us -> none  [one_axis_at_a_time(): return functools.reduce(lax.psum, axes, shard)]
    all_gather x3 -> x0, blocking collectives: 41.5 us -> none  [stacked_from(): parts = lax.all_gather(parts, axes[k])]
  transfers between devices with their start and end apart: 4 -> 0, of which waited for: 3 -> 0; matrix products, arithmetic and copies ran while one was open for 1% -> 0% of each run, Pallas kernels for 0% -> 0%
where the time goes in v1:
time: 77.8 us; the launch traced here: 77.7 us
  Pallas kernels  71.8 us (92%)
  local copies, waits for them, and re-layouts  5.21 us (7%)
    pallas_call x1, Pallas kernels, step(): pl.pallas_call(kernel, out_shape=(jax.ShapeDtypeStruct((8, 256), BF16), j...  71.8 us
    unnamed x10, local copies, waits for them, and re-layouts  5.21 us

profile of v1, /device:TPU:1, one launch (start us, length us, event | category | flops | bytes accessed | tf_op | source)
XLA Modules:
  0.0 77.7 jit_solution(12080967954172964848)
XLA Ops:
  0.6 71.8 %shard_map.174 = (bf16[8,256]{1,0:T(8,128)(2,1)}, f32[4,256,256]{2,1,0:T(8,128)}, f32[1024,256]{1,0:T(8,128)}, f32[4,256]{1,0:T(4,128)}) custom-call(bf16[8,256]{1,0:T(8,128)(2,1)} %tokens.1, s32[1,256]{1,0:T(1,128)} %bitcast.3, f32[32,128]{1,0:T(8,128)} %bitcast.2, bf16[2,4096]{1,0:T(2,128)(2,1)} %refs_2_.1, bf16[2,4096]{1,0:T(2,128)(2,1)} %refs_3_.1, ...), custom_call_target="tpu_custom_call" | custom-call | tf_op jit(solution)/shard_map/pallas_call | solution.py:406
  72.4 0.0 copy-start.2
  72.4 0.7 copy-done.2
  73.1 0.6 copy.23
  73.7 0.0 copy-start
  73.7 2.4 %copy.24 = f32[4,256,256]{2,1,0:T(8,128)} copy(f32[4,256,256]{2,1,0:T(8,128)} %get-tuple-element.9) | data formatting | bytes 2097152
  76.1 0.0 copy-done
  76.1 0.0 copy-start.1
  76.1 1.0 %copy.25 = f32[1024,256]{1,0:T(8,128)} copy(f32[1024,256]{1,0:T(8,128)S(1)} %copy-done) | data formatting | bytes 2097152
  77.1 0.0 copy-done.1
  77.1 0.6 copy.26
Async XLA Ops:
  72.4 0.7 copy-start.2
  73.7 2.4 %copy-start = (f32[1024,256]{1,0:T(8,128)S(1)}, f32[1024,256]{1,0:T(8,128)}, u32[]{:S(2)}) copy-start(f32[1024,256]{1,0:T(8,128)} %get-tuple-element.10) | copy-start | bytes 3145732
  76.1 1.0 %copy-start.1 = (f32[4,256]{1,0:T(4,128)S(1)}, f32[4,256]{1,0:T(4,128)}, u32[]{:S(2)}) copy-start(f32[4,256]{1,0:T(4,128)} %get-tuple-element.11) | copy-start | bytes 12292

commit v2 on v1

v2 whole, which is shorter than its diff:
```python
import jax
import jax.numpy as jnp
from jax import lax
from jax.experimental import pallas as pl
from jax.experimental.pallas import tpu as pltpu
from jax.sharding import PartitionSpec as P

DQK = 256
MOST_LEN = 3072
EPS = 1e-06
NZ, NY, NX, NC = 16, 4, 4, 2
CUBE = 4
D = 4096
F32 = jnp.float32
BF16 = jnp.bfloat16
MESH = pl.DeviceIdType.MESH


def kernel(*refs):
    sources, (rows_out, cells_v, norms_v, max_out), rest = refs[:15], refs[15:19], refs[19:]
    held, rest = rest[:12], rest[12:]
    body(sources, held, rows_out, cells_v, norms_v, max_out, *rest)


def body(
    sources,
    held,
    rows_out,
    cells_v,
    norms_v,
    max_out,
    tok,
    slices,
    rslices,
    wgot,
    rgot,
    wgate,
    gain_b,
    part,
    got,
    rpart,
    rgots,
    gbuf,
    kq,
    qf,
    kf,
    dec,
    fre,
    local_sem,
    z_s,
    z_r,
    a_s,
    a_r,
    w_s,
    w_r,
    wr_s,
    wr_r,
    p_s,
    p_r,
    qz_s,
    qz_r,
    kz_s,
    kz_r,
    qy_s,
    qy_r,
    qx_s,
    qx_r,
    qd_s,
    qd_r,
):
    me = lax.axis_index("tp")
    core = me % NC
    x = (me // NC) % NX
    y = (me // (NC * NX)) % NY
    z = me // (NC * NX * NY)
    head = z // CUBE
    zlo = z % CUBE
    other = 1 - core
    a = x * other + y * core
    r = y * other + x * core

    def device(zz, yy, xx, cc):
        return (((zz * NY + yy) * NX + xx) * NC + cc,)

    def on_line(cls, t, cc):
        return device(z, t * (1 - cls) + y * cls, x * (1 - cls) + t * cls, cc)

    def send(ref, dst, ss, rs, to):
        return pltpu.make_async_remote_copy(
            src_ref=ref, dst_ref=dst, send_sem=ss, recv_sem=rs, device_id=to, device_id_type=MESH
        )

    (where_ref, gain_ref, wq_ref, wk_ref, wv_ref, wo_ref, wi_ref, wf_ref) = held[:8]
    (bi_ref, bf_ref, wr_ref, maxima_ref) = held[8:]
    targets = (tok.at[z, a],) + held[:11] + (cells_v, norms_v, maxima_ref)
    loads = [
        pltpu.make_async_copy(source, target, local_sem.at[i])
        for i, (source, target) in enumerate(zip(sources, targets))
    ]
    for copy in loads:
        copy.start()

    barrier = pltpu.get_barrier_semaphore()

    def greet(to):
        pl.semaphore_signal(barrier, inc=1, device_id=to, device_id_type=MESH)

    @pl.loop(0, NZ - 1)
    def _(i):
        dz = 8 + ((i + 1) // 2) * (2 * (i % 2) - 1)
        greet(device((z + dz) % NZ, y, x, core))

    for d in range(1, 4):
        for c in range(NC):
            greet(device(z, (y + d) % NY, x, c))
            greet(device(z, y, (x + d) % NX, c))
    greet(device(z, y, x, other))
    for dz in range(1, CUBE):
        for dy in range(1, NY):
            greet(device(head * CUBE + (zlo + dz) % CUBE, (y + dy) % NY, x, core))
    pl.semaphore_wait(barrier, NZ - 1 + 12 + 1 + 9)

    def z_copy(n, dz):
        mine = tok.at[z, a] if n == 0 else gbuf.at[:, z, a, core]
        return send(mine, mine, z_s.at[n, dz], z_r.at[n, dz], device((z + dz) % NZ, y, x, core))

    def a_copy(n, d):
        mine = tok.at[:, a] if n == 0 else gbuf.at[:, :, a, core]
        to = on_line(other, (a + d) % 4, core)
        return send(mine, mine, a_s.at[n, d], a_r.at[n, d], to)

    def start_z(n):
        @pl.loop(0, NZ - 1)
        def _(i):
            dz = 8 + ((i + 1) // 2) * (2 * (i % 2) - 1)
            z_copy(n, dz).start()

    def finish_z(n):
        @pl.loop(1, NZ)
        def _(dz):
            z_copy(n, dz).wait_recv()

    loads[0].wait()
    start_z(0)

    for i in (3, 4, 5, 6, 7, 8, 11):
        loads[i].wait()
    rows = jnp.concatenate(
        [
            wq_ref[...].astype(F32),
            wk_ref[...].astype(F32),
            wv_ref[...].astype(F32),
            wo_ref[...].astype(F32),
            jnp.zeros((4, D), F32),
            wi_ref[...].astype(F32),
            wf_ref[...].astype(F32),
        ],
        axis=0,
    )
    read = wr_ref[...].astype(F32)
    for t in range(4):
        for p in range(NZ // 2):
            at = slice(128 * p, 128 * (p + 1))
            zs = (2 * p, 2 * p + 1)
            by_y = jnp.concatenate(
                [rows[:, zz * 256 + t * 64 : zz * 256 + t * 64 + 64] for zz in zs], axis=1
            )
            by_x = jnp.concatenate(
                [
                    rows[:, zz * 256 + yy * 64 + t * 16 : zz * 256 + yy * 64 + t * 16 + 16]
                    for zz in zs
                    for yy in range(4)
                ],
                axis=1,
            )
            for cls, piece in ((0, by_y), (1, by_x)):
                slices[cls, t, :, at] = piece[0:16].astype(BF16)
                wgate[cls, t, :, at] = piece[16:24].astype(BF16)
        for p in range(NZ // 4):
            at = slice(128 * p, 128 * (p + 1))
            zs = range(4 * p, 4 * p + 4)
            rslices[0, t, :, at] = jnp.concatenate(
                [read[:, zz * 128 + t * 32 : zz * 128 + t * 32 + 32] for zz in zs], axis=1
            ).astype(BF16)
            rslices[1, t, :, at] = jnp.concatenate(
                [
                    read[:, zz * 128 + yy * 32 + t * 8 : zz * 128 + yy * 32 + t * 8 + 8]
                    for zz in zs
                    for yy in range(4)
                ],
                axis=1,
            ).astype(BF16)

    loads[2].wait()
    gain_t = gain_ref[...].T
    for zz in range(NZ):
        gain_lo = gain_t[:, 2 * zz : 2 * zz + 1]
        gain_hi = gain_t[:, 2 * zz + 1 : 2 * zz + 2]
        gain_b[zz, 0:128] = jnp.broadcast_to(gain_lo, (128, 128))
        gain_b[zz, 128:256] = jnp.broadcast_to(gain_hi, (128, 128))

    def w_copy(cls, d):
        mine = y * (1 - cls) + x * cls
        t = (mine + d) % 4
        return send(
            slices.at[cls, t],
            wgot.at[mine, core],
            w_s.at[cls, d],
            w_r.at[mine, core],
            on_line(cls, t, cls),
        )

    def r_copy(cls, d):
        mine = y * (1 - cls) + x * cls
        t = (mine + d) % 4
        return send(
            rslices.at[cls, t],
            rgot.at[mine, core],
            wr_s.at[cls, d],
            wr_r.at[mine, core],
            on_line(cls, t, cls),
        )

    w_copy(other, 0).start()
    for d in (2, 1, 3):
        w_copy(core, d).start()
        w_copy(other, d).start()
    r_copy(other, 0).start()
    for d in (2, 1, 3):
        r_copy(core, d).start()
        r_copy(other, d).start()
    wgot[r, core] = slices[core, r]
    rgot[r, core] = rslices[core, r]
    for half in range(2):
        gbuf[half, :, :, other] = jnp.zeros((NZ, 4, 4, 128), BF16)

    finish_z(0)
    for d in (2, 1, 3):
        a_copy(0, d).start()

    def got_weights(sem, ref):
        for d in range(4):
            t = (r + d) % 4
            if d > 0:
                send(ref.at[t, core], ref.at[t, core], sem.at[t, core], sem.at[t, core], device(z, y, x, other)).wait_recv()
            send(ref.at[t, other], ref.at[t, other], sem.at[t, other], sem.at[t, other], device(z, y, x, other)).wait_recv()

    got_weights(w_r, wgot)
    for d in (1, 3, 2):
        a_copy(0, d).wait_recv()

    acc = jnp.zeros((128, 256), F32)
    gates = jnp.zeros((8, 256), F32)
    squares = jnp.zeros((8, 256), F32)
    first = core == 0
    for p in range(4):
        blocks = []
        for zz in range(4 * p, 4 * p + 4):
            for aa in range(4):
                t = tok[zz, aa].astype(F32)
                squares = squares + t * t
                row = (y * other + aa * core) * 64 + (aa * other + x * core) * 16 + core * 8
                g = gain_b[zz, pl.ds(pl.multiple_of(row, 8), 8)]
                t = t * jnp.concatenate([g, g], axis=1)
                none = jnp.zeros_like(t)
                blocks.append(jnp.where(first, t, none))
                blocks.append(jnp.where(first, none, t))
        normed = jnp.concatenate(blocks, axis=0).astype(BF16)
        at = slice(256 * p, 256 * (p + 1))
        w = wgot[:, :, :, at].reshape(128, 256)
        acc = acc + jnp.dot(w, normed, preferred_element_type=F32)
        gates = gates + jnp.dot(wgate[core, r, :, at], normed, preferred_element_type=F32)
    total = jnp.sum(squares, axis=0, keepdims=True)
    for t in range(4):
        for c in range(NC):
            at = (t * 2 + c) * 16
            part[t, c, 0:16] = acc[at : at + 16]
            part[t, c, 16:24] = gates
            part[t, c, 12:13] = total

    def p_copy(n, c, d):
        t = (r + d) % 4
        source = part if n == 0 else rpart
        target = got if n == 0 else rgots
        return send(
            source.at[t, c], target.at[core, r], p_s.at[n, c, d], p_r.at[n, core, r], on_line(core, t, c)
        )

    def start_p(n):
        for d in (2, 1, 3):
            p_copy(n, core, d).start()
            p_copy(n, other, d).start()
        p_copy(n, other, 0).start()

    def finish_p(n):
        ref = got if n == 0 else rgots
        for d in range(4):
            t = (r + d) % 4
            if d > 0:
                mine = ref.at[core, t]
                send(mine, mine, p_r.at[n, core, t], p_r.at[n, core, t], device(z, y, x, other)).wait_recv()
            t = (a + d) % 4
            mine = ref.at[other, t]
            send(mine, mine, p_r.at[n, other, t], p_r.at[n, other, t], device(z, y, x, other)).wait_recv()

    start_p(0)
    got[core, r] = part[r, core]
    for i in (1, 9, 10, 14):
        loads[i].wait()
    length = 1.0 + where_ref[...].astype(F32) / MOST_LEN
    finish_p(0)
    sums = got[0, 0]
    for t in range(1, 8):
        sums = sums + got[t // 4, t % 4]
    scale = lax.rsqrt(sums[12:13] / D + EPS)
    proj = sums * scale
    query = proj[0:2].astype(BF16)
    key = (proj[2:4] * DQK ** (-0.5)).astype(BF16)
    for half in range(2):
        kq[z, y, x, core, half] = key[:, 128 * half : 128 * (half + 1)]
        kq[z, y, x, core, 2 + half] = query[:, 128 * half : 128 * (half + 1)]

    def qz_copy(dz, dy):
        mine = kq.at[z, y, x, core]
        to = device(head * CUBE + (zlo + dz) % CUBE, (y + dy) % NY, x, core)
        return send(mine, mine, qz_s.at[dz, dy], qz_r.at[dz, dy], to)

    def kz_copy(dh, j):
        mine = kq.at[z, y, x, core, pl.ds(0, 2)]
        to = device(((head + dh) % 4) * CUBE + (zlo + j) % CUBE, y, x, core)
        return send(mine, mine, kz_s.at[dh, j], kz_r.at[dh, j], to)

    def zs_of(dh):
        return pl.ds(((head + 4 - dh) % 4) * CUBE, CUBE)

    def parts(dh):
        return pl.ds(0, 4 if dh == 0 else 2)

    def qy_copy(dh, d):
        mine = kq.at[zs_of(dh), y, x, core, parts(dh)]
        to = device(z, (y + d) % NY, x, core)
        return send(mine, mine, qy_s.at[dh, d], qy_r.at[dh, d], to)

    def qx_copy(dh, d):
        mine = kq.at[zs_of(dh), :, x, core, parts(dh)]
        to = device(z, y, (x + d) % NX, core)
        return send(mine, mine, qx_s.at[dh, d], qx_r.at[dh, d], to)

    def qd_copy(dh, d):
        this = kq.at[zs_of(dh), :, (x + NX - d) % NX, core, parts(dh)]
        to = device(z, y, x, other)
        return send(this, this, qd_s.at[dh, d], qd_r.at[dh, d], to)

    near = [(dz, dy) for dz in range(4) for dy in range(4) if dz or dy]
    for dz, dy in sorted(near, key=lambda at: (-(at[0] > 1) - (at[1] == 2), at)):
        qz_copy(dz, dy).start()
    for dh in (2, 1, 3):
        for j in range(CUBE):
            kz_copy(dh, j).start()

    value = proj[4:8]
    outgate = jax.nn.sigmoid(proj[8:12])
    for h in range(4):
        gate_in = proj[16 + h : 17 + h] + bi_ref[h]
        forget = proj[20 + h : 21 + h] + bf_ref[h]
        logf = (jnp.minimum(forget, 0.0) - jnp.log1p(jnp.exp(-jnp.abs(forget)))) * length
        held_max = logf + maxima_ref[h : h + 1]
        new_max = jnp.maximum(held_max, gate_in)
        max_out[h : h + 1] = new_max
        dec[h] = jnp.exp(held_max - new_max)
        fre[h] = jnp.exp(gate_in - new_max)

    for dz, dy in near:
        qz_copy(dz, dy).wait_recv()
    for d in (2, 1, 3):
        qx_copy(0, d).start()
    qd_copy(0, 0).start()
    for d in (1, 3, 2):
        qx_copy(0, d).wait_recv()
        qd_copy(0, d).start()
    for dh in range(1, 4):
        for j in range(CUBE):
            kz_copy(dh, j).wait_recv()
        for d in (2, 1, 3):
            qy_copy(dh, d).start()
    for d in range(4):
        qd_copy(0, d).wait_recv()

    for half in range(2):
        lanes = slice(128 * half, 128 * (half + 1))
        kf[:, lanes] = kq[zs_of(0), :, :, :, half].astype(F32).reshape(DQK, 128)
        qf[:, lanes] = kq[zs_of(0), :, :, :, 2 + half].astype(F32).reshape(DQK, 128)
    loads[12].wait()
    loads[13].wait()
    decay = dec[head]
    fresh = fre[head]
    fv = fresh * value

    def memory(i, carry):
        at = pl.ds(pl.multiple_of(i * 16, 16), 16)
        q, k = qf[at], kf[at]
        own = norms_v[pl.ds(pl.multiple_of(head * DQK + i * 16, 16), 16)]
        out = []
        for v in range(4):
            new = decay * cells_v[v, at] + fv[v : v + 1] * k
            cells_v[v, at] = new
            prod = q * new
            out.append(carry[v] + prod[0:8] + prod[8:16])
        prod = q * (decay * own + fresh * k)
        out.append(carry[4] + prod[0:8] + prod[8:16])
        return tuple(out)

    sums = lax.fori_loop(0, DQK // 16, memory, (jnp.zeros((8, 256), F32),) * 5)
    denom = jnp.sum(sums[4], axis=0, keepdims=True)
    numer = jnp.concatenate([jnp.sum(sums[v], axis=0, keepdims=True) for v in range(4)], axis=0)
    hidden = numer / jnp.maximum(jnp.abs(denom), 1.0)
    gated = (hidden * outgate).astype(BF16)
    for half in range(2):
        gbuf[half, z, a, core] = gated[:, 128 * half : 128 * (half + 1)]

    start_z(1)
    got_weights(wr_r, rgot)
    for dh in range(1, 4):
        for d in (1, 3, 2):
            qy_copy(dh, d).wait_recv()
        for d in (2, 1, 3):
            qx_copy(dh, d).start()
        qd_copy(dh, 0).start()
    finish_z(1)
    for d in (2, 1, 3):
        a_copy(1, d).start()
    for dh in range(1, 4):
        for d in (1, 3, 2):
            qx_copy(dh, d).wait_recv()
            qd_copy(dh, d).start()
    for d in (1, 3, 2):
        a_copy(1, d).wait_recv()
    w = rgot[...].reshape(64, 512)
    for half in range(2):
        g = gbuf[half].reshape(512, 128)
        mixed = jnp.dot(w, g, preferred_element_type=F32)
        for t in range(4):
            for c in range(NC):
                at = (t * 2 + c) * 8
                rpart[t, c, :, 128 * half : 128 * (half + 1)] = mixed[at : at + 8]
    start_p(1)
    rgots[core, r] = rpart[r, core]

    for dh in range(1, 4):
        for d in range(4):
            qd_copy(dh, d).wait_recv()

    @pl.loop(0, 4)
    def _(h):
        at = pl.ds(pl.multiple_of(h * DQK, DQK), DQK)
        for half in range(2):
            lanes = slice(128 * half, 128 * (half + 1))
            k = kq[pl.ds(h * CUBE, CUBE), :, :, :, half].astype(F32).reshape(DQK, 128)
            norms_v[at, lanes] = dec[h][:, lanes] * norms_v[at, lanes] + fre[h][:, lanes] * k

    finish_p(1)
    mixed = rgots[0, 0]
    for t in range(1, 8):
        mixed = mixed + rgots[t // 4, t % 4]
    rows_out[...] = (tok[z, a].astype(F32) + mixed).astype(BF16)

    for n in range(2):

        @pl.loop(1, NZ)
        def _(dz):
            z_copy(n, dz).wait_send()

        for d in range(1, 4):
            a_copy(n, d).wait_send()
            p_copy(n, core, d).wait_send()
            p_copy(n, other, d).wait_send()
        p_copy(n, other, 0).wait_send()
    for copy in (w_copy, r_copy):
        copy(other, 0).wait_send()
        for d in range(1, 4):
            copy(core, d).wait_send()
            copy(other, d).wait_send()
    for dz, dy in near:
        qz_copy(dz, dy).wait_send()
    for dh in range(4):
        for d in range(1, 4):
            qx_copy(dh, d).wait_send()
        for d in range(4):
            qd_copy(dh, d).wait_send()
    for dh in range(1, 4):
        for j in range(CUBE):
            kz_copy(dh, j).wait_send()
        for d in range(1, 4):
            qy_copy(dh, d).wait_send()


def put(*refs):
    sems = refs[8]
    copies = [pltpu.make_async_copy(refs[i], refs[4 + i], sems.at[i]) for i in range(4)]
    for copy in copies:
        copy.start()
    for copy in copies:
        copy.wait()


RESULTS = (((8, 256), BF16), ((4, 256, 256), F32), ((1024, 256), F32), ((4, 256), F32))


def step(
    tokens,
    positions,
    norm_gain,
    w_query,
    w_key,
    w_value,
    w_outgate,
    w_input,
    w_forget,
    bias_input,
    bias_forget,
    w_read,
    cells,
    norms,
    maxima,
):
    vmem = pl.BlockSpec(memory_space=pltpu.VMEM)
    hbm = pl.BlockSpec(memory_space=pltpu.HBM)
    dma = pltpu.SemaphoreType.DMA
    operands = (
        tokens,
        positions.reshape(1, 256),
        norm_gain.reshape(32, 128),
        w_query,
        w_key,
        w_value,
        w_outgate,
        w_input,
        w_forget,
        bias_input,
        bias_forget,
        w_read,
        cells,
        norms,
        maxima,
    )
    results = pl.pallas_call(
        kernel,
        out_shape=tuple(pltpu.VMEM(shape, kind) for shape, kind in RESULTS),
        in_specs=[hbm] * 15,
        out_specs=(vmem,) * 4,
        scratch_shapes=[
            pltpu.VMEM((1, 256), jnp.int32),
            pltpu.VMEM((32, 128), F32),
            pltpu.VMEM((2, D), BF16),
            pltpu.VMEM((2, D), BF16),
            pltpu.VMEM((4, D), BF16),
            pltpu.VMEM((4, D), BF16),
            pltpu.VMEM((4, D), BF16),
            pltpu.VMEM((4, D), BF16),
            pltpu.SMEM((4,), F32),
            pltpu.SMEM((4,), F32),
            pltpu.VMEM((8, 2048), BF16),
            pltpu.VMEM((4, 256), F32),
            pltpu.VMEM((NZ, 4, 8, 256), BF16),
            pltpu.VMEM((2, 4, 16, 1024), BF16),
            pltpu.VMEM((2, 4, 8, 512), BF16),
            pltpu.VMEM((4, 2, 16, 1024), BF16),
            pltpu.VMEM((4, 2, 8, 512), BF16),
            pltpu.VMEM((2, 4, 8, 1024), BF16),
            pltpu.VMEM((NZ, 256, 128), F32),
            pltpu.VMEM((4, 2, 24, 256), F32),
            pltpu.VMEM((2, 4, 24, 256), F32),
            pltpu.VMEM((4, 2, 8, 256), F32),
            pltpu.VMEM((2, 4, 8, 256), F32),
            pltpu.VMEM((2, NZ, 4, 2, 4, 128), BF16),
            pltpu.VMEM((NZ, NY, NX, NC, 4, 2, 128), BF16),
            pltpu.VMEM((256, 256), F32),
            pltpu.VMEM((256, 256), F32),
            pltpu.VMEM((4, 1, 256), F32),
            pltpu.VMEM((4, 1, 256), F32),
            dma((15,)),
            dma((2, 16)),
            dma((2, 16)),
            dma((2, 4)),
            dma((2, 4)),
            dma((2, 4)),
            dma((4, 2)),
            dma((2, 4)),
            dma((4, 2)),
            dma((2, 2, 4)),
            dma((2, 2, 4)),
            dma((4, 4)),
            dma((4, 4)),
            dma((4, 4)),
            dma((4, 4)),
            dma((4, 4)),
            dma((4, 4)),
            dma((4, 4)),
            dma((4, 4)),
            dma((4, 4)),
            dma((4, 4)),
        ],
        compiler_params=pltpu.CompilerParams(
            collective_id=0, has_side_effects=True, vmem_limit_bytes=40 * 1024 * 1024
        ),
    )(*[pltpu.with_memory_space_constraint(operand, pltpu.HBM) for operand in operands])
    return pl.pallas_call(
        put,
        out_shape=tuple(pltpu.HBM(shape, kind) for shape, kind in RESULTS),
        in_specs=[vmem] * 4,
        out_specs=(hbm,) * 4,
        scratch_shapes=[dma((4,))],
    )(*[pltpu.with_memory_space_constraint(result, pltpu.VMEM) for result in results])


def solution(mesh):
    return jax.shard_map(
        step,
        mesh=mesh,
        in_specs=(
            P("tp", None),
            P(),
            P(),
            P("tp", None),
            P("tp", None),
            P("tp", None),
            P("tp", None),
            P(),
            P(),
            P(),
            P(),
            P("tp", None),
            P("tp", None, None),
            P(),
            P(),
        ),
        out_specs=(P("tp", None), P("tp", None, None), P(), P()),
        check_vma=False,
    )
```

time: 77.8 us -> 63.2 us (0.81)
  Pallas kernels: 71.8 us -> 62.4 us
  local copies, waits for them, and re-layouts: 5.21 us -> 0 us
    pallas_call x1 -> x2, Pallas kernels: 71.8 us -> 62.4 us  [the longest x1 61 us: step(): pl.pallas_call(kernel, out_shape=tuple((pltpu.VMEM(shape, kind) for shape...]
    unnamed x10 -> x0, local copies, waits for them, and re-layouts: 5.21 us -> none
where the time goes in v2:
time: 63.2 us; the launch traced here: 63 us
  Pallas kernels  62.4 us (99%)
  between operations  0.65 us (1%)
    pallas_call x1, Pallas kernels, step(): pl.pallas_call(kernel, out_shape=tuple((pltpu.VMEM(shape, kind) for shape...  61 us
    pallas_call x1, Pallas kernels, step(): pl.pallas_call(put, out_shape=tuple((pltpu.HBM(shape, kind) for shape, ki...  1.36 us

profile of v2, /device:TPU:1, one launch (start us, length us, event | category | flops | bytes accessed | tf_op | source)
XLA Modules:
  0.0 63.0 jit_solution(14690123371307363820)
XLA Ops:
  0.6 61.0 %shard_map.174 = (bf16[8,256]{1,0:T(8,128)(2,1)S(1)}, f32[4,256,256]{2,1,0:T(8,128)S(1)}, f32[1024,256]{1,0:T(8,128)S(1)}, f32[4,256]{1,0:T(4,128)S(1)}) custom-call(bf16[8,256]{1,0:T(8,128)(2,1)} %refs_0_.1, s32[1,256]{1,0:T(1,128)} %bitcast.3, f32[32,128]{1,0:T(8,128)} %bitcast.2, bf16[2,4096]{1,0:T(2,128)(2,1)} %refs_3_.1, bf16[2,4096]{1,0:T(2,128)(2,1)} %refs_4_.1, ...), custom_call_target="tpu_custom_call" | custom-call | tf_op jit(solution)/shard_map/pallas_call | solution.py:546
  61.7 1.4 %shard_map.175 = (bf16[8,256]{1,0:T(8,128)(2,1)}, f32[4,256,256]{2,1,0:T(8,128)}, f32[1024,256]{1,0:T(8,128)}, f32[4,256]{1,0:T(4,128)}) custom-call(bf16[8,256]{1,0:T(8,128)(2,1)S(1)} %get-tuple-element.8.refs_0_, f32[4,256,256]{2,1,0:T(8,128)S(1)} %get-tuple-element.9.refs_1_, f32[1024,256]{1,0:T(8,128)S(1)} %get-tuple-element.10.refs_2_, ...), custom_call_target="tpu_custom_call" | custom-call | tf_op jit(solution)/shard_map/pallas_call | solution.py:607

commit v3 on v2

--- a/solution.py
+++ b/solution.py
@@ -30,6 +30,7 @@
     norms_v,
     max_out,
     tok,
+    rows_v,
     slices,
     rslices,
     wgot,
@@ -38,6 +39,8 @@
     gain_b,
     part,
     got,
+    lpart,
+    lgot,
     rpart,
     rgots,
     gbuf,
@@ -49,6 +52,8 @@
     local_sem,
     z_s,
     z_r,
+    gz_s,
+    gz_r,
     a_s,
     a_r,
     w_s,
@@ -92,7 +97,7 @@
 
     (where_ref, gain_ref, wq_ref, wk_ref, wv_ref, wo_ref, wi_ref, wf_ref) = held[:8]
     (bi_ref, bf_ref, wr_ref, maxima_ref) = held[8:]
-    targets = (tok.at[z, a],) + held[:11] + (cells_v, norms_v, maxima_ref)
+    targets = (tok.at[8, a],) + held[:11] + (cells_v, norms_v, maxima_ref)
     loads = [
         pltpu.make_async_copy(source, target, local_sem.at[i])
         for i, (source, target) in enumerate(zip(sources, targets))
@@ -105,70 +110,71 @@
     def greet(to):
         pl.semaphore_signal(barrier, inc=1, device_id=to, device_id_type=MESH)
 
-    @pl.loop(0, NZ - 1)
-    def _(i):
-        dz = 8 + ((i + 1) // 2) * (2 * (i % 2) - 1)
-        greet(device((z + dz) % NZ, y, x, core))
-
+    for dz in (4, -4, 3, -3, 2, -2, 1, -1):
+        greet(device((z + NZ + dz) % NZ, y, x, core))
     for d in range(1, 4):
         for c in range(NC):
             greet(device(z, (y + d) % NY, x, c))
             greet(device(z, y, (x + d) % NX, c))
     greet(device(z, y, x, other))
-    for dz in range(1, CUBE):
-        for dy in range(1, NY):
-            greet(device(head * CUBE + (zlo + dz) % CUBE, (y + dy) % NY, x, core))
-    pl.semaphore_wait(barrier, NZ - 1 + 12 + 1 + 9)
-
-    def z_copy(n, dz):
-        mine = tok.at[z, a] if n == 0 else gbuf.at[:, z, a, core]
-        return send(mine, mine, z_s.at[n, dz], z_r.at[n, dz], device((z + dz) % NZ, y, x, core))
+    pl.semaphore_wait(barrier, 8 + 12 + 1)
+
+    def near_copy(dz):
+        to = device((z + NZ + dz) % NZ, y, x, core)
+        return send(tok.at[8, a], tok.at[8 - dz, a], z_s.at[8 - dz], z_r.at[8 - dz], to)
+
+    def far_copy(dz):
+        source, target = (4, 4 - dz) if dz > 0 else (12, 12 - dz)
+        to = device((z + NZ + dz) % NZ, y, x, core)
+        return send(tok.at[source, a], tok.at[target, a], z_s.at[target], z_r.at[target], to)
 
     def a_copy(n, d):
-        mine = tok.at[:, a] if n == 0 else gbuf.at[:, :, a, core]
+        mine = tok.at[pl.ds((4, 0, 13)[n], (9, 4, 3)[n]), a]
         to = on_line(other, (a + d) % 4, core)
         return send(mine, mine, a_s.at[n, d], a_r.at[n, d], to)
 
-    def start_z(n):
-        @pl.loop(0, NZ - 1)
-        def _(i):
-            dz = 8 + ((i + 1) // 2) * (2 * (i % 2) - 1)
-            z_copy(n, dz).start()
-
-    def finish_z(n):
-        @pl.loop(1, NZ)
-        def _(dz):
-            z_copy(n, dz).wait_recv()
+    def gz_copy(dz):
+        mine = gbuf.at[:, z, a, core]
+        return send(mine, mine, gz_s.at[dz], gz_r.at[dz], device((z + dz) % NZ, y, x, core))
+
+    def ga_copy(d):
+        mine = gbuf.at[:, :, a, core]
+        to = on_line(other, (a + d) % 4, core)
+        return send(mine, mine, a_s.at[3, d], a_r.at[3, d], to)
 
     loads[0].wait()
-    start_z(0)
+    nearest = (4, -4, 3, -3, 2, -2, 1, -1)
+    farther = (4, -3, 3, -2, 2, -1, 1)
+    for dz in nearest:
+        near_copy(dz).start()
 
     for i in (3, 4, 5, 6, 7, 8, 11):
         loads[i].wait()
-    rows = jnp.concatenate(
+    rows_v[...] = jnp.concatenate(
         [
             wq_ref[...].astype(F32),
             wk_ref[...].astype(F32),
+            jnp.zeros((4, D), F32),
             wv_ref[...].astype(F32),
             wo_ref[...].astype(F32),
-            jnp.zeros((4, D), F32),
             wi_ref[...].astype(F32),
             wf_ref[...].astype(F32),
         ],
         axis=0,
     )
     read = wr_ref[...].astype(F32)
-    for t in range(4):
-        for p in range(NZ // 2):
-            at = slice(128 * p, 128 * (p + 1))
-            zs = (2 * p, 2 * p + 1)
-            by_y = jnp.concatenate(
-                [rows[:, zz * 256 + t * 64 : zz * 256 + t * 64 + 64] for zz in zs], axis=1
-            )
+    for p in range(NZ // 2):
+        at = slice(128 * p, 128 * (p + 1))
+        pair = []
+        for s in (2 * p, 2 * p + 1):
+            zz = (z + s + 8) % NZ
+            pair.append(rows_v[:, pl.ds(pl.multiple_of(zz * 256, 256), 256)])
+        for t in range(4):
+            by_y = jnp.concatenate([w[:, t * 64 : t * 64 + 64] for w in pair], axis=1)
             by_x = jnp.concatenate(
                 [
-                    rows[:, zz * 256 + yy * 64 + t * 16 : zz * 256 + yy * 64 + t * 16 + 16]
-                    for zz in zs
+                    w[:, yy * 64 + t * 16 : yy * 64 + t * 16 + 16]
+                    for w in pair
                     for yy in range(4)
                 ],
                 axis=1,
@@ -176,6 +182,7 @@
             for cls, piece in ((0, by_y), (1, by_x)):
                 slices[cls, t, :, at] = piece[0:16].astype(BF16)
                 wgate[cls, t, :, at] = piece[16:24].astype(BF16)
+    for t in range(4):
         for p in range(NZ // 4):
             at = slice(128 * p, 128 * (p + 1))
             zs = range(4 * p, 4 * p + 4)
@@ -234,9 +241,22 @@
     for half in range(2):
         gbuf[half, :, :, other] = jnp.zeros((NZ, 4, 4, 128), BF16)
 
-    finish_z(0)
+    for dz in (4, -4):
+        near_copy(dz).wait_recv()
+    for dz in farther:
+        far_copy(dz).start()
+    for dz in (1, -1, 2, -2, 3, -3):
+        near_copy(dz).wait_recv()
     for d in (2, 1, 3):
         a_copy(0, d).start()
+    for dz in (1, 2, 3, 4):
+        far_copy(dz).wait_recv()
+    for d in (2, 1, 3):
+        a_copy(1, d).start()
+    for dz in (-1, -2, -3):
+        far_copy(dz).wait_recv()
+    for d in (2, 1, 3):
+        a_copy(2, d).start()
 
     def got_weights(sem, ref):
         for d in range(4):
@@ -246,8 +266,9 @@
             send(ref.at[t, other], ref.at[t, other], sem.at[t, other], sem.at[t, other], device(z, y, x, other)).wait_recv()
 
     got_weights(w_r, wgot)
-    for d in (1, 3, 2):
-        a_copy(0, d).wait_recv()
+    for n in range(3):
+        for d in (1, 3, 2):
+            a_copy(n, d).wait_recv()
 
     acc = jnp.zeros((128, 256), F32)
     gates = jnp.zeros((8, 256), F32)
@@ -260,7 +281,7 @@
                 t = tok[zz, aa].astype(F32)
                 squares = squares + t * t
                 row = (y * other + aa * core) * 64 + (aa * other + x * core) * 16 + core * 8
-                g = gain_b[zz, pl.ds(pl.multiple_of(row, 8), 8)]
+                g = gain_b[(z + zz + 8) % NZ, pl.ds(pl.multiple_of(row, 8), 8)]
                 t = t * jnp.concatenate([g, g], axis=1)
                 none = jnp.zeros_like(t)
                 blocks.append(jnp.where(first, t, none))
@@ -274,14 +295,12 @@
     for t in range(4):
         for c in range(NC):
             at = (t * 2 + c) * 16
-            part[t, c, 0:16] = acc[at : at + 16]
-            part[t, c, 16:24] = gates
-            part[t, c, 12:13] = total
+            part[t, c, 0:4] = acc[at : at + 4]
+            part[t, c, 4:5] = total
 
     def p_copy(n, c, d):
         t = (r + d) % 4
-        source = part if n == 0 else rpart
-        target = got if n == 0 else rgots
+        source, target = ((part, got), (lpart, lgot), (rpart, rgots))[n]
         return send(
             source.at[t, c], target.at[core, r], p_s.at[n, c, d], p_r.at[n, core, r], on_line(core, t, c)
         )
@@ -293,7 +312,7 @@
         p_copy(n, other, 0).start()
 
     def finish_p(n):
-        ref = got if n == 0 else rgots
+        ref = (got, lgot, rgots)[n]
         for d in range(4):
             t = (r + d) % 4
             if d > 0:
@@ -304,7 +323,14 @@
             send(mine, mine, p_r.at[n, other, t], p_r.at[n, other, t], device(z, y, x, other)).wait_recv()
 
     start_p(0)
+    for t in range(4):
+        for c in range(NC):
+            at = (t * 2 + c) * 16
+            lpart[t, c, 0:8] = acc[at + 8 : at + 16]
+            lpart[t, c, 8:16] = gates
+    start_p(1)
     got[core, r] = part[r, core]
+    lgot[core, r] = lpart[r, core]
     for i in (1, 9, 10, 14):
         loads[i].wait()
     length = 1.0 + where_ref[...].astype(F32) / MOST_LEN
@@ -312,8 +338,8 @@
     sums = got[0, 0]
     for t in range(1, 8):
         sums = sums + got[t // 4, t % 4]
-    scale = lax.rsqrt(sums[12:13] / D + EPS)
-    proj = sums * scale
+    scale = lax.rsqrt(sums[4:5] / D + EPS)
+    proj = sums[0:4] * scale
     query = proj[0:2].astype(BF16)
     key = (proj[2:4] * DQK ** (-0.5)).astype(BF16)
     for half in range(2):
@@ -358,11 +384,16 @@
         for j in range(CUBE):
             kz_copy(dh, j).start()
 
-    value = proj[4:8]
-    outgate = jax.nn.sigmoid(proj[8:12])
+    finish_p(1)
+    sums = lgot[0, 0]
+    for t in range(1, 8):
+        sums = sums + lgot[t // 4, t % 4]
+    proj = sums * scale
+    value = proj[0:4]
+    outgate = jax.nn.sigmoid(proj[4:8])
     for h in range(4):
-        gate_in = proj[16 + h : 17 + h] + bi_ref[h]
-        forget = proj[20 + h : 21 + h] + bf_ref[h]
+        gate_in = proj[8 + h : 9 + h] + bi_ref[h]
+        forget = proj[12 + h : 13 + h] + bf_ref[h]
         logf = (jnp.minimum(forget, 0.0) - jnp.log1p(jnp.exp(-jnp.abs(forget)))) * length
         held_max = logf + maxima_ref[h : h + 1]
         new_max = jnp.maximum(held_max, gate_in)
@@ -418,7 +449,8 @@
     for half in range(2):
         gbuf[half, z, a, core] = gated[:, 128 * half : 128 * (half + 1)]
 
-    start_z(1)
+    for i in range(NZ - 1):
+        gz_copy(8 + ((i + 1) // 2) * (2 * (i % 2) - 1)).start()
     got_weights(wr_r, rgot)
     for dh in range(1, 4):
         for d in (1, 3, 2):
@@ -426,15 +458,16 @@
         for d in (2, 1, 3):
             qx_copy(dh, d).start()
         qd_copy(dh, 0).start()
-    finish_z(1)
+    for dz in range(1, NZ):
+        gz_copy(dz).wait_recv()
     for d in (2, 1, 3):
-        a_copy(1, d).start()
+        ga_copy(d).start()
     for dh in range(1, 4):
         for d in (1, 3, 2):
             qx_copy(dh, d).wait_recv()
             qd_copy(dh, d).start()
     for d in (1, 3, 2):
-        a_copy(1, d).wait_recv()
+        ga_copy(d).wait_recv()
     w = rgot[...].reshape(64, 512)
     for half in range(2):
         g = gbuf[half].reshape(512, 128)
@@ -443,7 +476,7 @@
             for c in range(NC):
                 at = (t * 2 + c) * 8
                 rpart[t, c, :, 128 * half : 128 * (half + 1)] = mixed[at : at + 8]
-    start_p(1)
+    start_p(2)
     rgots[core, r] = rpart[r, core]
 
     for dh in range(1, 4):
@@ -458,18 +491,21 @@
             k = kq[pl.ds(h * CUBE, CUBE), :, :, :, half].astype(F32).reshape(DQK, 128)
             norms_v[at, lanes] = dec[h][:, lanes] * norms_v[at, lanes] + fre[h][:, lanes] * k
 
-    finish_p(1)
+    finish_p(2)
     mixed = rgots[0, 0]
     for t in range(1, 8):
         mixed = mixed + rgots[t // 4, t % 4]
-    rows_out[...] = (tok[z, a].astype(F32) + mixed).astype(BF16)
-
-    for n in range(2):
-
-        @pl.loop(1, NZ)
-        def _(dz):
-            z_copy(n, dz).wait_send()
-
+    rows_out[...] = (tok[8, a].astype(F32) + mixed).astype(BF16)
+
+    for dz in nearest:
+        near_copy(dz).wait_send()
+    for dz in farther:
+        far_copy(dz).wait_send()
+    for dz in range(1, NZ):
+        gz_copy(dz).wait_send()
+    for d in range(1, 4):
+        ga_copy(d).wait_send()
+    for n in range(3):
         for d in range(1, 4):
             a_copy(n, d).wait_send()
             p_copy(n, core, d).wait_send()
@@ -562,14 +598,17 @@
             pltpu.VMEM((8, 2048), BF16),
             pltpu.VMEM((4, 256), F32),
             pltpu.VMEM((NZ, 4, 8, 256), BF16),
+            pltpu.VMEM((24, D), F32),
             pltpu.VMEM((2, 4, 16, 1024), BF16),
             pltpu.VMEM((2, 4, 8, 512), BF16),
             pltpu.VMEM((4, 2, 16, 1024), BF16),
             pltpu.VMEM((4, 2, 8, 512), BF16),
             pltpu.VMEM((2, 4, 8, 1024), BF16),
             pltpu.VMEM((NZ, 256, 128), F32),
-            pltpu.VMEM((4, 2, 24, 256), F32),
-            pltpu.VMEM((2, 4, 24, 256), F32),
+            pltpu.VMEM((4, 2, 8, 256), F32),
+            pltpu.VMEM((2, 4, 8, 256), F32),
+            pltpu.VMEM((4, 2, 16, 256), F32),
+            pltpu.VMEM((2, 4, 16, 256), F32),
             pltpu.VMEM((4, 2, 8, 256), F32),
             pltpu.VMEM((2, 4, 8, 256), F32),
             pltpu.VMEM((2, NZ, 4, 2, 4, 128), BF16),
@@ -579,16 +618,18 @@
             pltpu.VMEM((4, 1, 256), F32),
             pltpu.VMEM((4, 1, 256), F32),
             dma((15,)),
-            dma((2, 16)),
-            dma((2, 16)),
-            dma((2, 4)),
-            dma((2, 4)),
+            dma((16,)),
+            dma((16,)),
+            dma((16,)),
+            dma((16,)),
+            dma((4, 4)),
+            dma((4, 4)),
             dma((2, 4)),
             dma((4, 2)),
             dma((2, 4)),
             dma((4, 2)),
-            dma((2, 2, 4)),
-            dma((2, 2, 4)),
+            dma((3, 2, 4)),
+            dma((3, 2, 4)),
             dma((4, 4)),
             dma((4, 4)),
             dma((4, 4)),

time: 63.2 us -> 61.3 us (0.970)
  Pallas kernels: 62.4 us -> 60.5 us
    pallas_call x1, Pallas kernels: 61 us -> 59.1 us  [step(): pl.pallas_call(kernel, out_shape=tuple((pltpu.VMEM(shape, kind) for shape...]
where the time goes in v3:
time: 61.3 us; the launch traced here: 61.1 us
  Pallas kernels  60.5 us (99%)
  between operations  0.65 us (1%)
    pallas_call x1, Pallas kernels, step(): pl.pallas_call(kernel, out_shape=tuple((pltpu.VMEM(shape, kind) for shape...  59.1 us
    pallas_call x1, Pallas kernels, step(): pl.pallas_call(put, out_shape=tuple((pltpu.HBM(shape, kind) for shape, ki...  1.36 us

profile of v3, /device:TPU:1, one launch (start us, length us, event | category | flops | bytes accessed | tf_op | source)
XLA Modules:
  0.0 61.1 jit_solution(18329946546098881185)
XLA Ops:
  0.6 59.1 %shard_map.174 = (bf16[8,256]{1,0:T(8,128)(2,1)S(1)}, f32[4,256,256]{2,1,0:T(8,128)S(1)}, f32[1024,256]{1,0:T(8,128)S(1)}, f32[4,256]{1,0:T(4,128)S(1)}) custom-call(bf16[8,256]{1,0:T(8,128)(2,1)} %refs_0_.1, s32[1,256]{1,0:T(1,128)} %bitcast.3, f32[32,128]{1,0:T(8,128)} %bitcast.2, bf16[2,4096]{1,0:T(2,128)(2,1)} %refs_3_.1, bf16[2,4096]{1,0:T(2,128)(2,1)} %refs_4_.1, ...), custom_call_target="tpu_custom_call" | custom-call | tf_op jit(solution)/shard_map/pallas_call | solution.py:582
  59.8 1.4 %shard_map.175 = (bf16[8,256]{1,0:T(8,128)(2,1)}, f32[4,256,256]{2,1,0:T(8,128)}, f32[1024,256]{1,0:T(8,128)}, f32[4,256]{1,0:T(4,128)}) custom-call(bf16[8,256]{1,0:T(8,128)(2,1)S(1)} %get-tuple-element.8.refs_0_, f32[4,256,256]{2,1,0:T(8,128)S(1)} %get-tuple-element.9.refs_1_, f32[1024,256]{1,0:T(8,128)S(1)} %get-tuple-element.10.refs_2_, ...), custom_call_target="tpu_custom_call" | custom-call | tf_op jit(solution)/shard_map/pallas_call | solution.py:648

commit v4 on v3

v4 whole, which is shorter than its diff:
```python
import jax
import jax.numpy as jnp
from jax import lax
from jax.experimental import pallas as pl
from jax.experimental.pallas import tpu as pltpu
from jax.sharding import PartitionSpec as P

DQK = 256
MOST_LEN = 3072
EPS = 1e-06
NZ, NY, NX, NC = 16, 4, 4, 2
CUBE = 4
D = 4096
F32 = jnp.float32
BF16 = jnp.bfloat16
MESH = pl.DeviceIdType.MESH


def kernel(*refs):
    sources, (rows_out, cells_v, norms_v, max_out), rest = refs[:15], refs[15:19], refs[19:]
    held, rest = rest[:12], rest[12:]
    body(sources, held, rows_out, cells_v, norms_v, max_out, *rest)


def body(
    sources,
    held,
    rows_out,
    cells_v,
    norms_v,
    max_out,
    tok,
    rows_v,
    slices,
    rslices,
    wgot,
    rgot,
    wgate,
    gain_b,
    part,
    got,
    lpart,
    lgot,
    rpart,
    rgots,
    gbuf,
    kq,
    dec,
    fre,
    local_sem,
    z_s,
    z_r,
    a_s,
    a_r,
    w_s,
    w_r,
    p_s,
    p_r,
    q_s,
    q_r,
    qx_r,
):
    me = lax.axis_index("tp")
    core = me % NC
    x = (me // NC) % NX
    y = (me // (NC * NX)) % NY
    z = me // (NC * NX * NY)
    head = z // CUBE
    zlo = z % CUBE
    other = 1 - core
    a = x * other + y * core
    r = y * other + x * core

    def device(zz, yy, xx, cc):
        return (((zz * NY + yy) * NX + xx) * NC + cc,)

    def on_line(cls, t, cc):
        return device(z, t * (1 - cls) + y * cls, x * (1 - cls) + t * cls, cc)

    def send(ref, dst, ss, rs, to):
        return pltpu.make_async_remote_copy(
            src_ref=ref, dst_ref=dst, send_sem=ss, recv_sem=rs, device_id=to, device_id_type=MESH
        )

    (where_ref, gain_ref, wq_ref, wk_ref, wv_ref, wo_ref, wi_ref, wf_ref) = held[:8]
    (bi_ref, bf_ref, wr_ref, maxima_ref) = held[8:]
    targets = (tok.at[8, a],) + held[:11] + (cells_v, norms_v, maxima_ref)
    groups = (0, 2, 1, 1, 1, 1, 1, 1, 1, 3, 4, 1, 5, 6, 7)
    for source, target, group in zip(sources, targets, groups):
        pltpu.make_async_copy(source, target, local_sem.at[group]).start()

    def loaded(i, ref=None):
        target = targets[i] if ref is None else ref
        pltpu.make_async_copy(target, target, local_sem.at[groups[i]]).wait()

    partner = device(z, y, x, other)

    def arrived(sem, ref):
        send(ref, ref, sem, sem, partner).wait_recv()

    def left(sem, ref):
        send(ref, ref, sem, sem, partner).wait_send()

    barrier = pltpu.get_barrier_semaphore()

    def greet(to):
        pl.semaphore_signal(barrier, inc=1, device_id=to, device_id_type=MESH)

    for dz in (4, -4, 3, -3, 2, -2, 1, -1):
        greet(device((z + NZ + dz) % NZ, y, x, core))
    for d in range(1, 4):
        for c in range(NC):
            greet(device(z, (y + d) % NY, x, c))
            greet(device(z, y, (x + d) % NX, c))
    greet(partner)
    pl.semaphore_wait(barrier, 8 + 12 + 1)

    def near_copy(dz):
        to = device((z + NZ + dz) % NZ, y, x, core)
        group = 0 if dz == 4 else 1 if dz == -4 else 2
        return send(tok.at[8, a], tok.at[8 - dz, a], z_s.at[0], z_r.at[group], to)

    def far_copy(dz):
        source, target, group = (4, 4 - dz, 3) if dz > 0 else (12, 12 - dz, 4)
        to = device((z + NZ + dz) % NZ, y, x, core)
        return send(tok.at[source, a], tok.at[target, a], z_s.at[0], z_r.at[group], to)

    def a_copy(n, d):
        mine = tok.at[pl.ds((4, 0, 13)[n], (9, 4, 3)[n]), a]
        to = on_line(other, (a + d) % 4, core)
        return send(mine, mine, a_s.at[0], a_r.at[0], to)

    def gz_copy(dz):
        mine = gbuf.at[:, z, a, core]
        return send(mine, mine, z_s.at[1], z_r.at[5], device((z + dz) % NZ, y, x, core))

    def ga_copy(d):
        mine = gbuf.at[:, :, a, core]
        to = on_line(other, (a + d) % 4, core)
        return send(mine, mine, a_s.at[1], a_r.at[1], to)

    loaded(0)
    nearest = (4, -4, 3, -3, 2, -2, 1, -1)
    farther = (4, -3, 3, -2, 2, -1, 1)
    for dz in nearest:
        near_copy(dz).start()

    loaded(2, gain_b.at[pl.ds(0, 13), pl.ds(0, 32)])
    rows_v[...] = jnp.concatenate(
        [
            wq_ref[...].astype(F32),
            wk_ref[...].astype(F32),
            jnp.zeros((4, D), F32),
            wv_ref[...].astype(F32),
            wo_ref[...].astype(F32),
            wi_ref[...].astype(F32),
            wf_ref[...].astype(F32),
        ],
        axis=0,
    )
    read = wr_ref[...].astype(F32)
    for p in range(NZ // 2):
        at = slice(128 * p, 128 * (p + 1))
        pair = []
        for s in (2 * p, 2 * p + 1):
            zz = (z + s + 8) % NZ
            pair.append(rows_v[:, pl.ds(pl.multiple_of(zz * 256, 256), 256)])
        for t in range(4):
            by_y = jnp.concatenate([w[:, t * 64 : t * 64 + 64] for w in pair], axis=1)
            by_x = jnp.concatenate(
                [
                    w[:, yy * 64 + t * 16 : yy * 64 + t * 16 + 16]
                    for w in pair
                    for yy in range(4)
                ],
                axis=1,
            )
            for cls, piece in ((0, by_y), (1, by_x)):
                slices[cls * 4 + t, :, at] = piece[0:16].astype(BF16)
                wgate[cls * 4 + t, :, at] = piece[16:24].astype(BF16)
    for t in range(4):
        for p in range(NZ // 4):
            at = slice(128 * p, 128 * (p + 1))
            zs = range(4 * p, 4 * p + 4)
            rslices[t, :, at] = jnp.concatenate(
                [read[:, zz * 128 + t * 32 : zz * 128 + t * 32 + 32] for zz in zs], axis=1
            ).astype(BF16)
            rslices[4 + t, :, at] = jnp.concatenate(
                [
                    read[:, zz * 128 + yy * 32 + t * 8 : zz * 128 + yy * 32 + t * 8 + 8]
                    for zz in zs
                    for yy in range(4)
                ],
                axis=1,
            ).astype(BF16)

    gain_t = gain_ref[...].T
    for zz in range(NZ):
        gain_lo = gain_t[:, 2 * zz : 2 * zz + 1]
        gain_hi = gain_t[:, 2 * zz + 1 : 2 * zz + 2]
        gain_b[zz, 0:128] = jnp.broadcast_to(gain_lo, (128, 128))
        gain_b[zz, 128:256] = jnp.broadcast_to(gain_hi, (128, 128))

    def w_copy(cls, d):
        mine = y * (1 - cls) + x * cls
        t = (mine + d) % 4
        to = on_line(cls, t, cls)
        return send(
            slices.at[cls * 4 + t], wgot.at[mine * 2 + core], w_s.at[0], w_r.at[0], to
        )

    def r_copy(cls, d):
        mine = y * (1 - cls) + x * cls
        t = (mine + d) % 4
        to = on_line(cls, t, cls)
        return send(
            rslices.at[cls * 4 + t], rgot.at[mine * 2 + core], w_s.at[1], w_r.at[1], to
        )

    w_copy(other, 0).start()
    for d in (2, 1, 3):
        w_copy(core, d).start()
        w_copy(other, d).start()
    r_copy(other, 0).start()
    for d in (2, 1, 3):
        r_copy(core, d).start()
        r_copy(other, d).start()
    wgot[r * 2 + core] = slices[core * 4 + r]
    rgot[r * 2 + core] = rslices[core * 4 + r]
    for half in range(2):
        gbuf[half, :, :, other] = jnp.zeros((NZ, 4, 4, 128), BF16)

    arrived(z_r.at[0], tok.at[4, a])
    arrived(z_r.at[1], tok.at[12, a])
    for dz in farther:
        far_copy(dz).start()
    arrived(z_r.at[2], tok.at[pl.ds(5, 6), a])
    for d in (2, 1, 3):
        a_copy(0, d).start()
    arrived(z_r.at[3], tok.at[pl.ds(0, 4), a])
    for d in (2, 1, 3):
        a_copy(1, d).start()
    arrived(z_r.at[4], tok.at[pl.ds(13, 3), a])
    for d in (2, 1, 3):
        a_copy(2, d).start()

    arrived(w_r.at[0], wgot.at[pl.ds(0, 7)])
    arrived(a_r.at[0], tok.at[:, pl.ds(0, 3)])

    acc = jnp.zeros((128, 256), F32)
    gates = jnp.zeros((8, 256), F32)
    squares = jnp.zeros((8, 256), F32)
    first = core == 0
    for p in range(4):
        blocks = []
        for zz in range(4 * p, 4 * p + 4):
            for aa in range(4):
                t = tok[zz, aa].astype(F32)
                squares = squares + t * t
                row = (y * other + aa * core) * 64 + (aa * other + x * core) * 16 + core * 8
                g = gain_b[(z + zz + 8) % NZ, pl.ds(pl.multiple_of(row, 8), 8)]
                t = t * jnp.concatenate([g, g], axis=1)
                none = jnp.zeros_like(t)
                blocks.append(jnp.where(first, t, none))
                blocks.append(jnp.where(first, none, t))
        normed = jnp.concatenate(blocks, axis=0).astype(BF16)
        at = slice(256 * p, 256 * (p + 1))
        w = wgot[:, :, at].reshape(128, 256)
        acc = acc + jnp.dot(w, normed, preferred_element_type=F32)
        gates = gates + jnp.dot(wgate[core * 4 + r, :, at], normed, preferred_element_type=F32)
    total = jnp.sum(squares, axis=0, keepdims=True)
    for t in range(4):
        for c in range(NC):
            at = (t * 2 + c) * 16
            part[t * 2 + c, 0:4] = acc[at : at + 4]
            part[t * 2 + c, 4:5] = total

    def p_copy(n, c, d):
        t = (r + d) % 4
        source, target = ((part, got), (lpart, lgot), (rpart, rgots))[n]
        to = on_line(core, t, c)
        return send(source.at[t * 2 + c], target.at[core * 4 + r], p_s.at[n], p_r.at[n], to)

    def start_p(n):
        for d in (2, 1, 3):
            p_copy(n, core, d).start()
            p_copy(n, other, d).start()
        p_copy(n, other, 0).start()

    def finish_p(n):
        arrived(p_r.at[n], (got, lgot, rgots)[n].at[pl.ds(0, 7)])

    start_p(0)
    for t in range(4):
        for c in range(NC):
            at = (t * 2 + c) * 16
            lpart[t * 2 + c, 0:8] = acc[at + 8 : at + 16]
            lpart[t * 2 + c, 8:16] = gates
    start_p(1)
    got[core * 4 + r] = part[r * 2 + core]
    lgot[core * 4 + r] = lpart[r * 2 + core]
    for i in (1, 9, 10, 14):
        loaded(i)
    length = 1.0 + where_ref[...].astype(F32) / MOST_LEN
    finish_p(0)
    sums = got[0]
    for t in range(1, 8):
        sums = sums + got[t]
    scale = lax.rsqrt(sums[4:5] / D + EPS)
    proj = sums[0:4] * scale
    query = proj[0:2].astype(BF16)
    key = (proj[2:4] * DQK ** (-0.5)).astype(BF16)
    for half in range(2):
        kq[core, z, r, a, half] = key[:, 128 * half : 128 * (half + 1)]
        kq[core, z, r, a, 2 + half] = query[:, 128 * half : 128 * (half + 1)]

    def place(zz, tr, ta):
        return device(zz, tr * other + ta * core, ta * other + tr * core, core)

    def zs_of(dh):
        return pl.ds(((head + 4 - dh) % 4) * CUBE, CUBE)

    def parts(dh):
        return pl.ds(0, 4 if dh == 0 else 2)

    def qz_copy(dz, dr):
        mine = kq.at[core, z, r, a]
        to = place(head * CUBE + (zlo + dz) % CUBE, (r + dr) % 4, a)
        return send(mine, mine, q_s.at[0], q_r.at[0], to)

    def kz_copy(dh, j):
        mine = kq.at[core, z, r, a, pl.ds(0, 2)]
        to = place(((head + dh) % 4) * CUBE + (zlo + j) % CUBE, r, a)
        return send(mine, mine, q_s.at[1], q_r.at[1], to)

    def qy_copy(dh, d):
        mine = kq.at[core, zs_of(dh), r, a, parts(dh)]
        return send(mine, mine, q_s.at[2], q_r.at[2], place(z, (r + d) % 4, a))

    def qx_copy(dh, d):
        mine = kq.at[core, zs_of(dh), :, a, parts(dh)]
        if dh == 0:
            ss, rs = q_s.at[3], qx_r.at[d]
        else:
            ss, rs = q_s.at[4], q_r.at[4]
        return send(mine, mine, ss, rs, place(z, r, (a + d) % 4))

    def qd_copy(dh, d):
        this = kq.at[core, zs_of(dh), :, (a + 4 - d) % 4, parts(dh)]
        n = 5 if dh == 0 else 6
        return send(this, this, q_s.at[n], q_r.at[n], partner)

    def some(n):
        return (
            kq.at[0, pl.ds(0, 15), 0, 0],
            kq.at[0, pl.ds(0, 12), 0, 0, pl.ds(0, 2)],
            kq.at[0, pl.ds(0, 9), :, 0, pl.ds(0, 2)],
            kq.at[0, pl.ds(0, 12), :, 0],
            kq.at[0, pl.ds(0, 9), :, :, pl.ds(0, 2)],
            kq.at[0, :, :, 0],
            kq.at[0, pl.ds(0, 12), :, :, pl.ds(0, 2)],
        )[n]

    near = [(dz, dy) for dz in range(4) for dy in range(4) if dz or dy]
    for dz, dy in sorted(near, key=lambda at: (-(at[0] > 1) - (at[1] == 2), at)):
        qz_copy(dz, dy).start()
    for dh in (2, 1, 3):
        for j in range(CUBE):
            kz_copy(dh, j).start()

    finish_p(1)
    sums = lgot[0]
    for t in range(1, 8):
        sums = sums + lgot[t]
    proj = sums * scale
    value = proj[0:4]
    outgate = jax.nn.sigmoid(proj[4:8])
    for h in range(4):
        gate_in = proj[8 + h : 9 + h] + bi_ref[h]
        forget = proj[12 + h : 13 + h] + bf_ref[h]
        logf = (jnp.minimum(forget, 0.0) - jnp.log1p(jnp.exp(-jnp.abs(forget)))) * length
        held_max = logf + maxima_ref[h : h + 1]
        new_max = jnp.maximum(held_max, gate_in)
        max_out[h : h + 1] = new_max
        dec[h] = jnp.exp(held_max - new_max)
        fre[h] = jnp.exp(gate_in - new_max)

    arrived(q_r.at[0], some(0))
    for d in (2, 1, 3):
        qx_copy(0, d).start()
    qd_copy(0, 0).start()
    for d in (1, 3, 2):
        qx_copy(0, d).wait_recv()
        qd_copy(0, d).start()
    arrived(q_r.at[1], some(1))
    for dh in range(1, 4):
        for d in (2, 1, 3):
            qy_copy(dh, d).start()
    arrived(q_r.at[5], some(5))

    loaded(12)
    loaded(13)

    def rows_of(zz, yy, part):
        halves = []
        for half in range(2):
            g = 2 * part + half
            both = jnp.stack([kq[0, zz, yy, :, g], kq[1, zz, :, yy, g]], axis=1)
            halves.append(both.astype(F32).reshape(16, 128))
        return jnp.concatenate(halves, axis=1)

    decay = dec[head]
    fresh = fre[head]
    fv = fresh * value

    def memory(i, carry):
        at = pl.ds(pl.multiple_of(i * 16, 16), 16)
        zz, yy = head * CUBE + i // 4, i % 4
        q, k = rows_of(zz, yy, 1), rows_of(zz, yy, 0)
        own = norms_v[pl.ds(pl.multiple_of(head * DQK + i * 16, 16), 16)]
        out = []
        for v in range(4):
            new = decay * cells_v[v, at] + fv[v : v + 1] * k
            cells_v[v, at] = new
            prod = q * new
            out.append(carry[v] + prod[0:8] + prod[8:16])
        prod = q * (decay * own + fresh * k)
        out.append(carry[4] + prod[0:8] + prod[8:16])
        return tuple(out)

    sums = lax.fori_loop(0, DQK // 16, memory, (jnp.zeros((8, 256), F32),) * 5)
    denom = jnp.sum(sums[4], axis=0, keepdims=True)
    numer = jnp.concatenate([jnp.sum(sums[v], axis=0, keepdims=True) for v in range(4)], axis=0)
    hidden = numer / jnp.maximum(jnp.abs(denom), 1.0)
    gated = (hidden * outgate).astype(BF16)
    for half in range(2):
        gbuf[half, z, a, core] = gated[:, 128 * half : 128 * (half + 1)]

    for i in range(NZ - 1):
        gz_copy(8 + ((i + 1) // 2) * (2 * (i % 2) - 1)).start()
    arrived(w_r.at[1], rgot.at[pl.ds(0, 7)])
    arrived(q_r.at[2], some(2))
    for dh in range(1, 4):
        for d in (2, 1, 3):
            qx_copy(dh, d).start()
        qd_copy(dh, 0).start()
    arrived(z_r.at[5], gbuf.at[:, pl.ds(0, 15), 0, 0])
    for d in (2, 1, 3):
        ga_copy(d).start()
    arrived(q_r.at[4], some(4))
    for dh in range(1, 4):
        for d in (1, 3, 2):
            qd_copy(dh, d).start()
    arrived(a_r.at[1], gbuf.at[:, :, pl.ds(0, 3), 0])
    w = rgot[...].reshape(64, 512)
    for half in range(2):
        g = gbuf[half].reshape(512, 128)
        mixed = jnp.dot(w, g, preferred_element_type=F32)
        for t in range(4):
            for c in range(NC):
                at = (t * 2 + c) * 8
                rpart[t * 2 + c, :, 128 * half : 128 * (half + 1)] = mixed[at : at + 8]
    start_p(2)
    rgots[core * 4 + r] = rpart[r * 2 + core]

    arrived(q_r.at[6], some(6))

    @pl.loop(0, 64)
    def _(i):
        h = i // 16
        at = pl.ds(pl.multiple_of(i * 16, 16), 16)
        norms_v[at] = dec[h] * norms_v[at] + fre[h] * rows_of(i // 4, i % 4, 0)

    finish_p(2)
    mixed = rgots[0]
    for t in range(1, 8):
        mixed = mixed + rgots[t]
    rows_out[...] = (tok[8, a].astype(F32) + mixed).astype(BF16)

    left(z_s.at[0], tok.at[pl.ds(0, 15), 0])
    left(z_s.at[1], gbuf.at[:, pl.ds(0, 15), 0, 0])
    left(a_s.at[0], tok.at[:, pl.ds(0, 3)])
    left(a_s.at[1], gbuf.at[:, :, pl.ds(0, 3), 0])
    left(w_s.at[0], slices.at[pl.ds(0, 7)])
    left(w_s.at[1], rslices.at[pl.ds(0, 7)])
    for n, ref in enumerate((part, lpart, rpart)):
        left(p_s.at[n], ref.at[pl.ds(0, 7)])
    for n in range(7):
        left(q_s.at[n], some(n))


def put(*refs):
    sems = refs[8]
    copies = [pltpu.make_async_copy(refs[i], refs[4 + i], sems.at[i]) for i in range(4)]
    for copy in copies:
        copy.start()
    for copy in copies:
        copy.wait()


RESULTS = (((8, 256), BF16), ((4, 256, 256), F32), ((1024, 256), F32), ((4, 256), F32))


def step(
    tokens,
    positions,
    norm_gain,
    w_query,
    w_key,
    w_value,
    w_outgate,
    w_input,
    w_forget,
    bias_input,
    bias_forget,
    w_read,
    cells,
    norms,
    maxima,
):
    vmem = pl.BlockSpec(memory_space=pltpu.VMEM)
    hbm = pl.BlockSpec(memory_space=pltpu.HBM)
    dma = pltpu.SemaphoreType.DMA
    operands = (
        tokens,
        positions.reshape(1, 256),
        norm_gain.reshape(32, 128),
        w_query,
        w_key,
        w_value,
        w_outgate,
        w_input,
        w_forget,
        bias_input,
        bias_forget,
        w_read,
        cells,
        norms,
        maxima,
    )
    results = pl.pallas_call(
        kernel,
        out_shape=tuple(pltpu.VMEM(shape, kind) for shape, kind in RESULTS),
        in_specs=[hbm] * 15,
        out_specs=(vmem,) * 4,
        scratch_shapes=[
            pltpu.VMEM((1, 256), jnp.int32),
            pltpu.VMEM((32, 128), F32),
            pltpu.VMEM((2, D), BF16),
            pltpu.VMEM((2, D), BF16),
            pltpu.VMEM((4, D), BF16),
            pltpu.VMEM((4, D), BF16),
            pltpu.VMEM((4, D), BF16),
            pltpu.VMEM((4, D), BF16),
            pltpu.SMEM((4,), F32),
            pltpu.SMEM((4,), F32),
            pltpu.VMEM((8, 2048), BF16),
            pltpu.VMEM((4, 256), F32),
            pltpu.VMEM((NZ, 4, 8, 256), BF16),
            pltpu.VMEM((24, D), F32),
            pltpu.VMEM((8, 16, 1024), BF16),
            pltpu.VMEM((8, 8, 512), BF16),
            pltpu.VMEM((8, 16, 1024), BF16),
            pltpu.VMEM((8, 8, 512), BF16),
            pltpu.VMEM((8, 8, 1024), BF16),
            pltpu.VMEM((NZ, 256, 128), F32),
            pltpu.VMEM((8, 8, 256), F32),
            pltpu.VMEM((8, 8, 256), F32),
            pltpu.VMEM((8, 16, 256), F32),
            pltpu.VMEM((8, 16, 256), F32),
            pltpu.VMEM((8, 8, 256), F32),
            pltpu.VMEM((8, 8, 256), F32),
            pltpu.VMEM((2, NZ, 4, 2, 4, 128), BF16),
            pltpu.VMEM((2, NZ, 4, 4, 4, 2, 128), BF16),
            pltpu.VMEM((4, 1, 256), F32),
            pltpu.VMEM((4, 1, 256), F32),
            dma((8,)),
            dma((2,)),
            dma((6,)),
            dma((2,)),
            dma((2,)),
            dma((2,)),
            dma((2,)),
            dma((3,)),
            dma((3,)),
            dma((7,)),
            dma((7,)),
            dma((4,)),
        ],
        compiler_params=pltpu.CompilerParams(
            collective_id=0, has_side_effects=True, vmem_limit_bytes=40 * 1024 * 1024
        ),
    )(*[pltpu.with_memory_space_constraint(operand, pltpu.HBM) for operand in operands])
    return pl.pallas_call(
        put,
        out_shape=tuple(pltpu.HBM(shape, kind) for shape, kind in RESULTS),
        in_specs=[vmem] * 4,
        out_specs=(hbm,) * 4,
        scratch_shapes=[dma((4,))],
    )(*[pltpu.with_memory_space_constraint(result, pltpu.VMEM) for result in results])


def solution(mesh):
    return jax.shard_map(
        step,
        mesh=mesh,
        in_specs=(
            P("tp", None),
            P(),
            P(),
            P("tp", None),
            P("tp", None),
            P("tp", None),
            P("tp", None),
            P(),
            P(),
            P(),
            P(),
            P("tp", None),
            P("tp", None, None),
            P(),
            P(),
        ),
        out_specs=(P("tp", None), P("tp", None, None), P(), P()),
        check_vma=False,
    )
```

time: 61.3 us -> 58.5 us (0.954)
  Pallas kernels: 60.5 us -> 57.8 us
    pallas_call x1, Pallas kernels: 59.1 us -> 56.4 us  [step(): pl.pallas_call(kernel, out_shape=tuple((pltpu.VMEM(shape, kind) for shape...]
where the time goes in v4:
time: 58.5 us; the launch traced here: 58.4 us
  Pallas kernels  57.8 us (99%)
  between operations  0.65 us (1%)
    pallas_call x1, Pallas kernels, step(): pl.pallas_call(kernel, out_shape=tuple((pltpu.VMEM(shape, kind) for shape...  56.4 us
    pallas_call x1, Pallas kernels, step(): pl.pallas_call(put, out_shape=tuple((pltpu.HBM(shape, kind) for shape, ki...  1.36 us

profile of v4, /device:TPU:1, one launch (start us, length us, event | category | flops | bytes accessed | tf_op | source)
XLA Modules:
  0.0 58.4 jit_solution(9130087225330245101)
XLA Ops:
  0.6 56.4 %shard_map.174 = (bf16[8,256]{1,0:T(8,128)(2,1)S(1)}, f32[4,256,256]{2,1,0:T(8,128)S(1)}, f32[1024,256]{1,0:T(8,128)S(1)}, f32[4,256]{1,0:T(4,128)S(1)}) custom-call(bf16[8,256]{1,0:T(8,128)(2,1)} %refs_0_.1, s32[1,256]{1,0:T(1,128)} %bitcast.3, f32[32,128]{1,0:T(8,128)} %bitcast.2, bf16[2,4096]{1,0:T(2,128)(2,1)} %refs_3_.1, bf16[2,4096]{1,0:T(2,128)(2,1)} %refs_4_.1, ...), custom_call_target="tpu_custom_call" | custom-call | tf_op jit(solution)/shard_map/pallas_call | solution.py:541
  57.0 1.4 %shard_map.175 = (bf16[8,256]{1,0:T(8,128)(2,1)}, f32[4,256,256]{2,1,0:T(8,128)}, f32[1024,256]{1,0:T(8,128)}, f32[4,256]{1,0:T(4,128)}) custom-call(bf16[8,256]{1,0:T(8,128)(2,1)S(1)} %get-tuple-element.8.refs_0_, f32[4,256,256]{2,1,0:T(8,128)S(1)} %get-tuple-element.9.refs_1_, f32[1024,256]{1,0:T(8,128)S(1)} %get-tuple-element.10.refs_2_, ...), custom_call_target="tpu_custom_call" | custom-call | tf_op jit(solution)/shard_map/pallas_call | solution.py:594

commit v5 on v4

--- a/solution.py
+++ b/solution.py
@@ -58,6 +58,7 @@
     p_r,
     q_s,
     q_r,
+    qz_r,
     qx_r,
 ):
     me = lax.axis_index("tp")
@@ -106,42 +107,46 @@
     def greet(to):
         pl.semaphore_signal(barrier, inc=1, device_id=to, device_id_type=MESH)
 
-    for dz in (4, -4, 3, -3, 2, -2, 1, -1):
+    for dz in (3, -3, 2, -2, 1, -1):
         greet(device((z + NZ + dz) % NZ, y, x, core))
     for d in range(1, 4):
         for c in range(NC):
             greet(device(z, (y + d) % NY, x, c))
             greet(device(z, y, (x + d) % NX, c))
     greet(partner)
-    pl.semaphore_wait(barrier, 8 + 12 + 1)
+    pl.semaphore_wait(barrier, 6 + 12 + 1)
 
     def near_copy(dz):
         to = device((z + NZ + dz) % NZ, y, x, core)
-        group = 0 if dz == 4 else 1 if dz == -4 else 2
+        group = 0 if dz == 3 else 1 if dz == -3 else 2
         return send(tok.at[8, a], tok.at[8 - dz, a], z_s.at[0], z_r.at[group], to)
 
     def far_copy(dz):
-        source, target, group = (4, 4 - dz, 3) if dz > 0 else (12, 12 - dz, 4)
+        source, target, group = (5, 5 - dz, 3) if dz > 0 else (11, 11 - dz, 4)
         to = device((z + NZ + dz) % NZ, y, x, core)
         return send(tok.at[source, a], tok.at[target, a], z_s.at[0], z_r.at[group], to)
 
     def a_copy(n, d):
-        mine = tok.at[pl.ds((4, 0, 13)[n], (9, 4, 3)[n]), a]
+        mine = tok.at[pl.ds((5, 0, 12)[n], (7, 5, 4)[n]), a]
         to = on_line(other, (a + d) % 4, core)
         return send(mine, mine, a_s.at[0], a_r.at[0], to)
 
     def gz_copy(dz):
-        mine = gbuf.at[:, z, a, core]
-        return send(mine, mine, z_s.at[1], z_r.at[5], device((z + dz) % NZ, y, x, core))
-
-    def ga_copy(d):
-        mine = gbuf.at[:, :, a, core]
+        to = device((z + NZ + dz) % NZ, y, x, core)
+        group = 5 if -4 <= dz <= 4 else 6
+        return send(
+            gbuf.at[:, 8, a, core], gbuf.at[:, 8 - dz, a, core], z_s.at[1], z_r.at[group], to
+        )
+
+    def ga_copy(n, d):
+        mine = gbuf.at[:, pl.ds((4, 0, 13)[n], (9, 4, 3)[n]), a, core]
         to = on_line(other, (a + d) % 4, core)
         return send(mine, mine, a_s.at[1], a_r.at[1], to)
 
     loaded(0)
-    nearest = (4, -4, 3, -3, 2, -2, 1, -1)
-    farther = (4, -3, 3, -2, 2, -1, 1)
+    nearest = (3, -3, 2, -2, 1, -1)
+    spread = (8, 7, -7, 6, -6, 5, -5, 4, -4, 3, -3, 2, -2, 1, -1)
+    farther = (5, -4, 4, -3, 3, -2, 2, -1, 1)
     for dz in nearest:
         near_copy(dz).start()
 
@@ -158,7 +163,6 @@
         ],
         axis=0,
     )
-    read = wr_ref[...].astype(F32)
     for p in range(NZ // 2):
         at = slice(128 * p, 128 * (p + 1))
         pair = []
@@ -178,19 +182,18 @@
             for cls, piece in ((0, by_y), (1, by_x)):
                 slices[cls * 4 + t, :, at] = piece[0:16].astype(BF16)
                 wgate[cls * 4 + t, :, at] = piece[16:24].astype(BF16)
-    for t in range(4):
-        for p in range(NZ // 4):
-            at = slice(128 * p, 128 * (p + 1))
-            zs = range(4 * p, 4 * p + 4)
+    for p in range(NZ // 4):
+        at = slice(128 * p, 128 * (p + 1))
+        four = []
+        for s in range(4 * p, 4 * p + 4):
+            zz = (z + s + 8) % NZ
+            four.append(wr_ref[:, pl.ds(pl.multiple_of(zz * 128, 128), 128)].astype(F32))
+        for t in range(4):
             rslices[t, :, at] = jnp.concatenate(
-                [read[:, zz * 128 + t * 32 : zz * 128 + t * 32 + 32] for zz in zs], axis=1
+                [w[:, t * 32 : t * 32 + 32] for w in four], axis=1
             ).astype(BF16)
             rslices[4 + t, :, at] = jnp.concatenate(
-                [
-                    read[:, zz * 128 + yy * 32 + t * 8 : zz * 128 + yy * 32 + t * 8 + 8]
-                    for zz in zs
-                    for yy in range(4)
-                ],
+                [w[:, yy * 32 + t * 8 : yy * 32 + t * 8 + 8] for w in four for yy in range(4)],
                 axis=1,
             ).astype(BF16)
 
@@ -230,17 +233,17 @@
     for half in range(2):
         gbuf[half, :, :, other] = jnp.zeros((NZ, 4, 4, 128), BF16)
 
-    arrived(z_r.at[0], tok.at[4, a])
-    arrived(z_r.at[1], tok.at[12, a])
+    arrived(z_r.at[0], tok.at[5, a])
+    arrived(z_r.at[1], tok.at[11, a])
     for dz in farther:
         far_copy(dz).start()
-    arrived(z_r.at[2], tok.at[pl.ds(5, 6), a])
+    arrived(z_r.at[2], tok.at[pl.ds(6, 4), a])
     for d in (2, 1, 3):
         a_copy(0, d).start()
-    arrived(z_r.at[3], tok.at[pl.ds(0, 4), a])
+    arrived(z_r.at[3], tok.at[pl.ds(0, 5), a])
     for d in (2, 1, 3):
         a_copy(1, d).start()
-    arrived(z_r.at[4], tok.at[pl.ds(13, 3), a])
+    arrived(z_r.at[4], tok.at[pl.ds(12, 4), a])
     for d in (2, 1, 3):
         a_copy(2, d).start()
 
@@ -326,7 +329,7 @@
     def qz_copy(dz, dr):
         mine = kq.at[core, z, r, a]
         to = place(head * CUBE + (zlo + dz) % CUBE, (r + dr) % 4, a)
-        return send(mine, mine, q_s.at[0], q_r.at[0], to)
+        return send(mine, mine, q_s.at[0], qz_r.at[dz], to)
 
     def kz_copy(dh, j):
         mine = kq.at[core, z, r, a, pl.ds(0, 2)]
@@ -337,13 +340,13 @@
         mine = kq.at[core, zs_of(dh), r, a, parts(dh)]
         return send(mine, mine, q_s.at[2], q_r.at[2], place(z, (r + d) % 4, a))
 
+    def q_plane(dz, d):
+        mine = kq.at[core, head * CUBE + (zlo + CUBE - dz) % CUBE, :, a]
+        return send(mine, mine, q_s.at[3], qx_r.at[d], place(z, r, (a + d) % 4))
+
     def qx_copy(dh, d):
         mine = kq.at[core, zs_of(dh), :, a, parts(dh)]
-        if dh == 0:
-            ss, rs = q_s.at[3], qx_r.at[d]
-        else:
-            ss, rs = q_s.at[4], q_r.at[4]
-        return send(mine, mine, ss, rs, place(z, r, (a + d) % 4))
+        return send(mine, mine, q_s.at[4], q_r.at[4], place(z, r, (a + d) % 4))
 
     def qd_copy(dh, d):
         this = kq.at[core, zs_of(dh), :, (a + 4 - d) % 4, parts(dh)]
@@ -385,12 +388,13 @@
         dec[h] = jnp.exp(held_max - new_max)
         fre[h] = jnp.exp(gate_in - new_max)
 
-    arrived(q_r.at[0], some(0))
-    for d in (2, 1, 3):
-        qx_copy(0, d).start()
+    for dz in (0, 1, 3, 2):
+        arrived(qz_r.at[dz], kq.at[0, pl.ds(0, 3 if dz == 0 else 4), 0, 0])
+        for d in (2, 1, 3):
+            q_plane(dz, d).start()
     qd_copy(0, 0).start()
     for d in (1, 3, 2):
-        qx_copy(0, d).wait_recv()
+        arrived(qx_r.at[d], kq.at[0, pl.ds(0, 4), :, 0])
         qd_copy(0, d).start()
     arrived(q_r.at[1], some(1))
     for dh in range(1, 4):
@@ -434,19 +438,23 @@
     hidden = numer / jnp.maximum(jnp.abs(denom), 1.0)
     gated = (hidden * outgate).astype(BF16)
     for half in range(2):
-        gbuf[half, z, a, core] = gated[:, 128 * half : 128 * (half + 1)]
-
-    for i in range(NZ - 1):
-        gz_copy(8 + ((i + 1) // 2) * (2 * (i % 2) - 1)).start()
+        gbuf[half, 8, a, core] = gated[:, 128 * half : 128 * (half + 1)]
+
+    for dz in spread:
+        gz_copy(dz).start()
     arrived(w_r.at[1], rgot.at[pl.ds(0, 7)])
     arrived(q_r.at[2], some(2))
     for dh in range(1, 4):
         for d in (2, 1, 3):
             qx_copy(dh, d).start()
         qd_copy(dh, 0).start()
-    arrived(z_r.at[5], gbuf.at[:, pl.ds(0, 15), 0, 0])
+    arrived(z_r.at[5], gbuf.at[:, pl.ds(0, 8), 0, 0])
     for d in (2, 1, 3):
-        ga_copy(d).start()
+        ga_copy(0, d).start()
+    arrived(z_r.at[6], gbuf.at[:, pl.ds(0, 7), 0, 0])
+    for n in (1, 2):
+        for d in (2, 1, 3):
+            ga_copy(n, d).start()
     arrived(q_r.at[4], some(4))
     for dh in range(1, 4):
         for d in (1, 3, 2):
@@ -576,7 +584,7 @@
             pltpu.VMEM((4, 1, 256), F32),
             dma((8,)),
             dma((2,)),
-            dma((6,)),
+            dma((7,)),
             dma((2,)),
             dma((2,)),
             dma((2,)),
@@ -585,6 +593,7 @@
             dma((3,)),
             dma((7,)),
             dma((7,)),
+            dma((4,)),
             dma((4,)),
         ],
         compiler_params=pltpu.CompilerParams(

time: 58.5 us -> 58 us (level)
  Pallas kernels: 57.8 us -> 57.2 us
where the time goes in v5:
time: 58 us; the launch traced here: 57.9 us
  Pallas kernels  57.2 us (99%)
  between operations  0.65 us (1%)
    pallas_call x1, Pallas kernels, step(): pl.pallas_call(kernel, out_shape=tuple((pltpu.VMEM(shape, kind) for shape...  55.9 us
    pallas_call x1, Pallas kernels, step(): pl.pallas_call(put, out_shape=tuple((pltpu.HBM(shape, kind) for shape, ki...  1.36 us

profile of v5, /device:TPU:1, one launch (start us, length us, event | category | flops | bytes accessed | tf_op | source)
XLA Modules:
  0.0 57.9 jit_solution(17058253608722567137)
XLA Ops:
  0.6 55.9 %shard_map.174 = (bf16[8,256]{1,0:T(8,128)(2,1)S(1)}, f32[4,256,256]{2,1,0:T(8,128)S(1)}, f32[1024,256]{1,0:T(8,128)S(1)}, f32[4,256]{1,0:T(4,128)S(1)}) custom-call(bf16[8,256]{1,0:T(8,128)(2,1)} %refs_0_.1, s32[1,256]{1,0:T(1,128)} %bitcast.3, f32[32,128]{1,0:T(8,128)} %bitcast.2, bf16[2,4096]{1,0:T(2,128)(2,1)} %refs_3_.1, bf16[2,4096]{1,0:T(2,128)(2,1)} %refs_4_.1, ...), custom_call_target="tpu_custom_call" | custom-call | tf_op jit(solution)/shard_map/pallas_call | solution.py:549
  56.5 1.4 %shard_map.175 = (bf16[8,256]{1,0:T(8,128)(2,1)}, f32[4,256,256]{2,1,0:T(8,128)}, f32[1024,256]{1,0:T(8,128)}, f32[4,256]{1,0:T(4,128)}) custom-call(bf16[8,256]{1,0:T(8,128)(2,1)S(1)} %get-tuple-element.8.refs_0_, f32[4,256,256]{2,1,0:T(8,128)S(1)} %get-tuple-element.9.refs_1_, f32[1024,256]{1,0:T(8,128)S(1)} %get-tuple-element.10.refs_2_, ...), custom_call_target="tpu_custom_call" | custom-call | tf_op jit(solution)/shard_map/pallas_call | solution.py:603
